TPU v7x, 512 devices: a whole 4x4x16 slice. The times are simulated.
512 devices in a mesh: sp: 64 (over z, y), tp: 8 (over x, core).
Axes of the slice: x: 4, y: 4, z: 16, core: 2. Of those that a mesh axis runs over, the one named last changes fastest.
Arguments:
- tokens: bfloat16 [24576, 2048], P(('sp', 'tp')), may hold values from -6 to 6
- norm_gain: float32 [2048], replicated, may hold values from 0.1 to 1.9
- conv_in_weight: bfloat16 [2048, 2048], P('sp', 'tp'), may hold values from -0.125 to 0.125
- conv_gate_weight: bfloat16 [2048, 2048], P('sp', 'tp'), may hold values from -0.125 to 0.125
- conv_taps: float32 [3, 2048], replicated, may hold values from -3 to 3
- query_weight: bfloat16 [2048, 1024], P('sp', 'tp'), may hold values from -0.125 to 0.125
- key_weight: bfloat16 [2048, 1024], P('sp', 'tp'), may hold values from -0.125 to 0.125
- value_weight: bfloat16 [2048, 2048], P('sp', 'tp'), may hold values from -0.125 to 0.125
- decay_down: bfloat16 [2048, 16], replicated, may hold values from -0.125 to 0.125
- decay_up: bfloat16 [16, 1024], replicated, may hold values from -1.5 to 1.5
- decay_bias: float32 [1024], replicated, may hold values from 0.2 to 10
- decay_extra: float32 [8, 24576], P('tp', 'sp'), may hold values from -2.2 to 0
- head_gain: float32 [2048], replicated, may hold values from 0.1 to 1.9
- conv_out_weight: bfloat16 [2048, 2048], P('tp', 'sp'), may hold values from -0.125 to 0.125
- value_out_weight: bfloat16 [2048, 2048], P('tp', 'sp'), may hold values from -0.125 to 0.125
Outputs:
- mixed: bfloat16 [24576, 2048], P(('sp', 'tp'))
All inputs are finite; a program needn't handle non-finite values.
Results may differ from a plain program's by a relative error of at most 0.02.
Values may be sent and summed in bfloat16 or wider, within the bound.
A program may use at most 64 MiB of HBM per device.

v0:
```python
import math

import jax
import jax.numpy as jnp
from jax import lax
from jax.sharding import Mesh
from jax.sharding import PartitionSpec as P

KEY_DIM = 128
VAL_DIM = 256
BLOCK = 64
SP = ("sp_0", "sp_1")
SP_TP = ("sp_0", "sp_1", "tp")


EPSILON = 1e-06


def nothing_yet(array, identity):
    return jax.tree.map(
        lambda part, zero: jnp.zeros_like(part) + jnp.asarray(zero, part.dtype), array, identity
    )


def prefix_by_axis(array, axes, combine, identity, reverse):
    before = start = nothing_yet(array, identity)
    subtotal = array
    for axis in reversed(axes):
        count, place = (lax.axis_size(axis), lax.axis_index(axis))
        pieces = jax.tree.map(
            lambda part, kind: lax.all_gather(part.astype(kind), axis),
            subtotal,
            (jnp.bfloat16, jnp.bfloat16),
        )
        inside, subtotal = (start, start)
        for k in reversed(range(count)) if reverse else range(count):
            passed = k > place if reverse else k < place
            subtotal = combine(
                subtotal, jax.tree.map(lambda part, own: part[k].astype(own.dtype), pieces, array)
            )
            inside = jax.tree.map(lambda new, old: jnp.where(passed, new, old), subtotal, inside)
        before = combine(inside, before)
    return before


def copy_for_each(array, axis):
    count = lax.axis_size(axis)
    return lax.all_to_all(
        jnp.broadcast_to(array[None], (count, *array.shape)), axis, 0, 0, tiled=True
    )


def joined_along(blocks, dim):
    blocks = jnp.moveaxis(blocks, 0, dim)
    dims = blocks.shape
    return blocks.reshape(*dims[:dim], dims[dim] * dims[dim + 1], *dims[dim + 2 :])


def gathered_copies(array, axis, dim):
    blocks = copy_for_each(array, axis)
    return joined_along(blocks, dim)


def rows_first(arrays, axis, dims):
    turned = [jnp.moveaxis(a, dim, 0) for a, dim in zip(arrays, dims)]
    widths = [t[0].size for t in turned]
    both = jnp.concatenate([t.reshape(-1, w) for t, w in zip(turned, widths)], axis=1)
    filled = lax.all_gather(both, axis, axis=0, tiled=True)
    blocks = jnp.split(filled, [sum(widths[:k]) for k in range(1, len(widths))], axis=1)
    return tuple(
        (
            jnp.moveaxis(b.reshape(-1, *t.shape[1:]), 0, dim)
            for b, t, dim in zip(blocks, turned, dims)
        )
    )


def padded_2(block, sides, width):
    for axis, dim in sides:
        count = lax.axis_size(axis)
        forward = [(i, i + 1) for i in range(count - 1)]
        backward = [(target, source) for source, target in forward]
        low = lax.ppermute(
            lax.slice_in_dim(block, block.shape[dim] - width, None, axis=dim), axis, forward
        )
        high = lax.ppermute(lax.slice_in_dim(block, 0, width, axis=dim), axis, backward)
        block = jnp.concatenate([low, block, high], axis=dim)
    return block


def cut_along(array, dim, count):
    before, after = (array.shape[:dim], array.shape[dim + 1 :])
    return jnp.moveaxis(array.reshape(*before, count, -1, *after), dim, 0)


def sum_at_owner(array, axis, dim):
    blocks = cut_along(array, dim, lax.axis_size(axis))
    arrived = lax.all_to_all(blocks, axis, split_axis=0, concat_axis=0, tiled=True)
    return arrived.astype(jnp.float32).sum(axis=0)


def rms_rows(inputs, scale_gain):
    floats = inputs.astype(jnp.float32)
    return (
        floats * lax.rsqrt(jnp.mean(floats * floats, axis=-1, keepdims=True) + EPSILON) * scale_gain
    )


def rounded(inputs):
    return lax.optimization_barrier(inputs.astype(jnp.bfloat16)).astype(jnp.float32)


def project(normed, weight):
    return jnp.dot(normed, weight, preferred_element_type=jnp.float32)


def chain_combine(earlier, later):
    return (earlier[0] * later[0], later[0][..., None] * earlier[1] + later[1])


def gla_heads(queries, key_rows, values, log_decay):
    length, head_count, key_dim = queries.shape
    val_dim = values.shape[-1]
    blocks = length // BLOCK
    query_float = queries.astype(jnp.float32).reshape(blocks, BLOCK, head_count, key_dim)
    key_float = key_rows.astype(jnp.float32).reshape(blocks, BLOCK, head_count, key_dim)
    value_float = values.astype(jnp.float32).reshape(blocks, BLOCK, head_count, val_dim)
    decay_blocks = log_decay.reshape(blocks, BLOCK, head_count, key_dim)
    cumul = jnp.cumsum(decay_blocks, axis=1)
    before = cumul - decay_blocks
    totals = cumul[:, -1]
    offsets = jnp.cumsum(totals, axis=0) - totals
    whole_decay = jnp.sum(totals, axis=0)
    element_indices = jnp.arange(BLOCK)
    lower_mask = element_indices[:, None] >= element_indices[None, :]
    fwd_query = query_float * jnp.exp(cumul)
    fwd_scores = jnp.einsum("nihd,njhd->nhij", fwd_query, key_float * jnp.exp(-cumul))
    fwd_scores = jnp.where(lower_mask, fwd_scores, 0.0)
    key_start = key_float * jnp.exp(before)
    back_scores = jnp.einsum("nihd,njhd->nhij", query_float * jnp.exp(-before), key_start)
    back_scores = jnp.where(lower_mask.T, back_scores, 0.0)
    within = jnp.einsum("nhij,njhe->nihe", fwd_scores + back_scores, value_float)
    fwd_inc = jnp.einsum(
        "njhd,njhe->nhde", key_float * jnp.exp(totals[:, None] - cumul), value_float
    )
    back_inc = jnp.einsum("njhd,njhe->nhde", key_start, value_float)
    tail_decay = jnp.exp(whole_decay[None] - offsets - totals)
    fwd_device = jnp.einsum("nhd,nhde->hde", tail_decay, fwd_inc)
    back_device = jnp.einsum("nhd,nhde->hde", jnp.exp(offsets), back_inc)
    identity = (jnp.ones_like(whole_decay), jnp.zeros_like(fwd_device))
    incoming_fwd = prefix_by_axis(
        (jnp.exp(whole_decay), fwd_device), SP, chain_combine, identity, False
    )[1]
    incoming_back = prefix_by_axis(
        (jnp.exp(whole_decay), back_device), SP, chain_combine, identity, True
    )[1]
    block_order = jnp.arange(blocks)
    earlier_mask = (block_order[:, None] > block_order[None, :])[:, :, None, None]
    gap_fwd = offsets[:, None] - offsets[None, :] - totals[None, :]
    weights_fwd = jnp.exp(jnp.where(earlier_mask, gap_fwd, -jnp.inf))
    starts_fwd = (
        jnp.einsum("bchd,chde->bhde", weights_fwd, fwd_inc)
        + jnp.exp(offsets)[..., None] * incoming_fwd[None]
    )
    later_mask = (block_order[:, None] < block_order[None, :])[:, :, None, None]
    gap_back = offsets[None, :] - offsets[:, None] - totals[:, None]
    weights_back = jnp.exp(jnp.where(later_mask, gap_back, -jnp.inf))
    next_back = (
        jnp.einsum("bchd,chde->bhde", weights_back, back_inc)
        + tail_decay[..., None] * incoming_back[None]
    )
    carried_terms = jnp.einsum("nihd,nhde->nihe", fwd_query, starts_fwd)
    carried_terms = carried_terms + jnp.einsum(
        "nihd,nhde->nihe", query_float * jnp.exp(totals[:, None] - before), next_back
    )
    return (within + carried_terms).reshape(length, head_count, val_dim)


def local(
    tokens,
    norm_gain,
    conv_in_weight,
    conv_gate_weight,
    conv_taps,
    query_weight,
    key_weight,
    value_weight,
    decay_down,
    decay_up,
    decay_bias,
    decay_extra,
    head_gain,
    conv_out_weight,
    value_out_weight,
):
    shard_index = lax.axis_index("tp")
    channels = conv_in_weight.shape[1]
    key_width = query_weight.shape[1]
    val_width = value_weight.shape[1]
    head_count = decay_extra.shape[0]
    gathered = gathered_copies(tokens, "tp", 0)
    normed = rms_rows(gathered, norm_gain).astype(jnp.bfloat16)
    length = normed.shape[0]
    gathered_weights = rows_first(
        (
            conv_in_weight,
            conv_gate_weight,
            query_weight,
            key_weight,
            value_weight,
            conv_out_weight,
            value_out_weight,
        ),
        SP,
        (0, 0, 0, 0, 0, 1, 1),
    )
    conv_pre = project(normed, gathered_weights[0])
    gate_pre = project(normed, gathered_weights[1])
    probe_before_norm = project(normed, gathered_weights[2])
    key_pre = project(normed, gathered_weights[3])
    value_pre = project(normed, gathered_weights[4])
    conv_out_full = gathered_weights[5]
    value_out_full = gathered_weights[6]
    conv_in = conv_pre.astype(jnp.bfloat16)
    padded = padded_2(conv_in, ((SP, 0),), 1).astype(jnp.float32)
    tap_slice = lax.dynamic_slice_in_dim(conv_taps, shard_index * channels, channels, 1)
    mixed_conv = (
        padded[:-2] * tap_slice[0] + padded[1:-1] * tap_slice[1] + padded[2:] * tap_slice[2]
    )
    conv_mixed = (mixed_conv * jax.nn.silu(rounded(gate_pre))).astype(jnp.bfloat16)
    queries = (probe_before_norm * (1.0 / math.sqrt(KEY_DIM))).astype(jnp.bfloat16)
    key_rows = key_pre.astype(jnp.bfloat16)
    values = value_pre.astype(jnp.bfloat16)
    low_rank = project(normed, decay_down).astype(jnp.bfloat16)
    key_offset = shard_index * key_width
    up_slice = lax.dynamic_slice_in_dim(decay_up, key_offset, key_width, 1)
    bias_slice = lax.dynamic_slice_in_dim(decay_bias, key_offset, key_width, 0)
    log_decay = jax.nn.log_sigmoid(project(low_rank, up_slice) + bias_slice) / 16.0
    log_decay = log_decay.reshape(length, head_count, KEY_DIM) + decay_extra.T[:, :, None]
    raw_mixed = gla_heads(
        queries.reshape(length, head_count, KEY_DIM),
        key_rows.reshape(length, head_count, KEY_DIM),
        values.reshape(length, head_count, VAL_DIM),
        log_decay,
    )
    gain_slice = lax.dynamic_slice_in_dim(head_gain, shard_index * val_width, val_width, 0).reshape(
        head_count, VAL_DIM
    )
    gla_mixed = rms_rows(raw_mixed, gain_slice).astype(jnp.bfloat16).reshape(length, val_width)
    mixed = sum_at_owner(
        (project(conv_mixed, conv_out_full) + project(gla_mixed, value_out_full)).astype(
            jnp.bfloat16
        ),
        "tp",
        0,
    )
    return mixed.astype(jnp.bfloat16)


def solution(mesh):
    torus = Mesh(mesh.devices.reshape(16, 4, mesh.shape["tp"]), ("sp_0", "sp_1", "tp"))
    return jax.shard_map(
        local,
        mesh=torus,
        in_specs=(
            P(SP_TP, None),
            P(),
            P(SP, "tp"),
            P(SP, "tp"),
            P(),
            P(SP, "tp"),
            P(SP, "tp"),
            P(SP, "tp"),
            P(),
            P(),
            P(),
            P("tp", SP),
            P(),
            P("tp", SP),
            P("tp", SP),
        ),
        out_specs=P(SP_TP, None),
        check_vma=False,
    )
```

profile of v0, /device:TPU:1, one launch (start us, length us, event | category | flops | bytes accessed | tf_op | source)
XLA Modules:
  0.0 377.7 jit_solution(13934947043964088281)
XLA Ops:
  6.5 0.8 constant_dynamic-update-slice_fusion.6
  7.3 0.7 constant_dynamic-update-slice_fusion.5
  8.0 0.7 constant_dynamic-update-slice_fusion.4
  8.7 0.7 constant_dynamic-update-slice_fusion.3
  9.4 0.7 constant_dynamic-update-slice_fusion.2
  10.1 0.7 constant_dynamic-update-slice_fusion.1
  10.9 0.7 constant_dynamic-update-slice_fusion
  12.3 2.3 broadcast_in_dim.36
  14.5 10.5 %all-to-all-start = ((bf16[8,48,2048]{2,1,0:T(8,128)(2,1)}), bf16[8,48,2048]{2,1,0:T(8,128)(2,1)S(1)}, u32[]{:S(2)}, u32[]{:S(2)}) async-start(bf16[8,48,2048]{2,1,0:T(8,128)(2,1)} %broadcast_in_dim.36), calls=%async_computation | async-start | bytes 3145728 | tf_op jit(solution)/shard_map/all_to_all | solution.py:48
  25.0 0.8 dynamic_slice.14
  25.8 19.8 %all-to-all-done = bf16[8,48,2048]{2,1,0:T(8,128)(2,1)S(1)} async-done(((bf16[8,48,2048]{2,1,0:T(8,128)(2,1)}), bf16[8,48,2048]{2,1,0:T(8,128)(2,1)S(1)}, u32[]{:S(2)}, u32[]{:S(2)}) %all-to-all-start) | async-done | bytes 1572896 | tf_op jit(solution)/shard_map/all_to_all | solution.py:48
  46.5 1.5 fusion.58
  48.6 5.9 %all-gather.3 = bf16[4,1,128]{2,1,0:T(2,128)(2,1)S(1)} all-gather(bf16[1,1,128]{2,1,0:T(2,128)(2,1)S(1)} %convert_bitcast_fusion), channel_id=2, replica_groups=mesh['sp_0'=16,'sp_1'=4,'tp'=8] {'sp_1'}, dimensions={0}, use_global_device_ids=true | all-gather | bytes 1280 | tf_op jit(solution)/shard_map/all_gather | solution.py:31
  55.1 105.2 %all-gather.8.cloned.1.call-done = bf16[2048,1536]{1,0:T(8,128)(2,1)} async-done(((bf16[32,1536]{1,0:T(8,128)(2,1)}), bf16[2048,1536]{1,0:T(8,128)(2,1)}) %all-gather.8.cloned.1.call-update) | async-done | bytes 6291472 | tf_op jit(solution)/shard_map/all_gather | solution.py:68
  160.4 1.6 convolution_convert_fusion.3
  162.0 1.8 convolution_convert_fusion
  164.5 9.4 %all-gather.2 = bf16[512,256]{1,0:T(8,128)(2,1)S(1)} all-gather(bf16[128,256]{1,0:T(8,128)(2,1)S(1)} %bitcast.364), channel_id=4, replica_groups=mesh['sp_0'=16,'sp_1'=4,'tp'=8] {'sp_1'}, dimensions={0}, use_global_device_ids=true | all-gather | bytes 327680 | tf_op jit(solution)/shard_map/all_gather | solution.py:31
  174.6 10.3 %all-gather.1 = bf16[512,256]{1,0:T(8,128)(2,1)S(1)} all-gather(bf16[128,256]{1,0:T(8,128)(2,1)S(1)} %bitcast.365), channel_id=3, replica_groups=mesh['sp_0'=16,'sp_1'=4,'tp'=8] {'sp_1'}, dimensions={0}, use_global_device_ids=true | all-gather | bytes 327680 | tf_op jit(solution)/shard_map/all_gather | solution.py:31
  184.9 0.8 fusion.87
  185.9 1.3 dynamic_slice.15
  188.3 0.9 constant_dynamic-slice_fusion
  189.2 0.7 copy.40
  189.9 0.7 copy.56
  190.7 0.7 copy.47
  191.4 0.7 copy.43
  192.1 0.7 copy.53
  192.9 20.4 %all_gather.43 = bf16[16,1,128]{2,1,0:T(2,128)(2,1)S(1)} all-gather(bf16[1,1,128]{2,1,0:T(2,128)(2,1)S(1)} %get-tuple-element.51), channel_id=1, replica_groups=mesh['sp_0'=16,'sp_1'=4,'tp'=8] {'sp_0'}, dimensions={0}, use_global_device_ids=true | all-gather | bytes 4352 | tf_op jit(solution)/shard_map/all_gather | solution.py:31
  213.3 19.5 %all_gather.39 = bf16[16,1,128]{2,1,0:T(2,128)(2,1)S(1)} all-gather(bf16[1,1,128]{2,1,0:T(2,128)(2,1)S(1)} %get-tuple-element.52), channel_id=1, replica_groups=mesh['sp_0'=16,'sp_1'=4,'tp'=8] {'sp_0'}, dimensions={0}, use_global_device_ids=true | all-gather | bytes 4352 | tf_op jit(solution)/shard_map/all_gather | solution.py:31
  235.1 1.8 convolution_convert_fusion.2
  236.9 1.9 collective-permute-start
  238.8 1.3 collective-permute-start.1
  240.1 1.6 fusion.8
  241.8 1.8 convolution_convert_fusion.1
  243.6 0.9 convolution_select_fusion.1
  244.5 1.9 fusion.17
  246.5 7.6 %all-gather.10.cloned.1.call-done = bf16[16,1,128,256]{3,2,1,0:T(8,128)(2,1)} async-done(((bf16[1,1,128,256]{3,2,1,0:T(8,128)(2,1)}), bf16[16,1,128,256]{3,2,1,0:T(8,128)(2,1)}) %all-gather.10.cloned.1.call-update) | async-done | bytes 1048592 | tf_op jit(solution)/shard_map/all_gather | solution.py:31
  254.1 2.0 fusion.86
  256.2 1.6 fusion.3
  257.8 1.0 fusion.22
  258.8 65.4 %all-gather.12.cloned.1.call-done = bf16[16,1,128,256]{3,2,1,0:T(8,128)(2,1)} async-done(((bf16[1,1,128,256]{3,2,1,0:T(8,128)(2,1)}), bf16[16,1,128,256]{3,2,1,0:T(8,128)(2,1)}) %all-gather.12.cloned.1.call-update) | async-done | bytes 1048592 | tf_op jit(solution)/shard_map/all_gather | solution.py:31
  324.2 2.0 fusion.79
  326.3 1.7 fusion.5
  328.1 1.0 convolution_add_fusion.1
  329.0 2.5 fusion.42
  331.6 1.1 fusion.41
  332.7 1.8 add_convert_fusion
  334.6 35.6 %all_to_all.10 = bf16[8,48,2048]{2,1,0:T(8,128)(2,1)S(1)} all-to-all(bf16[8,48,2048]{2,1,0:T(8,128)(2,1)S(1)} %bitcast.348), channel_id=1, replica_groups=mesh['sp_0'=16,'sp_1'=4,'tp'=8] {'tp'}, dimensions={0} | all-to-all | bytes 3145728 | tf_op jit(solution)/shard_map/all_to_all | solution.py:98
  370.2 0.9 reduce_sum.42
  (85 shorter events, 7.8 us)
Async XLA Ops:
  6.5 40.0 %copy-start = (bf16[2048,16]{0,1:T(8,128)(2,1)S(1)}, bf16[2048,16]{0,1:T(8,128)(2,1)}, u32[]{:S(2)}) copy-start(bf16[2048,16]{0,1:T(8,128)(2,1)} %param.23) | copy-start | bytes 196612
  6.5 153.8 %all-gather.8.cloned.1.call-start = ((), (), s32[]{:S(2)}) async-start(), calls=%async_computation.2 | async-start | bytes 6389760 | tf_op jit(solution)/shard_map/all_gather | solution.py:68
  11.6 0.7 copy-start.12
  14.5 11.2 %copy-start.20 = (f32[1,384]{1,0:T(1,128)S(1)}, f32[1,384]{1,0:T(1,128)}, u32[]{:S(2)}) copy-start(f32[1,384]{1,0:T(1,128)} %param.26) | copy-start | bytes 4612
  14.5 31.1 %all-to-all-start = ((bf16[8,48,2048]{2,1,0:T(8,128)(2,1)}), bf16[8,48,2048]{2,1,0:T(8,128)(2,1)S(1)}, u32[]{:S(2)}, u32[]{:S(2)}) async-start(bf16[8,48,2048]{2,1,0:T(8,128)(2,1)} %broadcast_in_dim.36), calls=%async_computation | async-start | bytes 3145728 | tf_op jit(solution)/shard_map/all_to_all | solution.py:48
  25.0 21.1 %copy-start.13 = (f32[2048]{0:T(1024)S(1)}, f32[2048]{0:T(1024)}, u32[]{:S(2)}) copy-start(f32[2048]{0:T(1024)} %param.16) | copy-start | bytes 24580
  25.0 229.1 %all-gather.10.cloned.1.call-start = ((), (), s32[]{:S(2)}) async-start(), calls=%async_computation.3 | async-start | bytes 1114112 | tf_op jit(solution)/shard_map/all_gather | solution.py:31
  48.1 115.7 %copy-start.1 = (f32[384,128]{1,0:T(8,128)}, f32[384,128]{1,0:T(8,128)S(1)}, u32[]{:S(2)}) copy-start(f32[384,128]{1,0:T(8,128)S(1)} %fusion.58) | copy-start | bytes 589828
  163.8 10.4 %copy-start.5 = (bf16[384,256]{1,0:T(8,128)(2,1)}, bf16[384,256]{1,0:T(8,128)(2,1)S(1)}, u32[]{:S(2)}) copy-start(bf16[384,256]{1,0:T(8,128)(2,1)S(1)} %convolution_convert_fusion) | copy-start | bytes 589828
  164.1 10.5 %copy-start.11 = (bf16[6,128,256]{2,1,0:T(8,128)(2,1)}, bf16[6,128,256]{2,1,0:T(8,128)(2,1)S(1)}, u32[]{:S(2)}) copy-start(bf16[6,128,256]{2,1,0:T(8,128)(2,1)S(1)} %fusion.89) | copy-start | bytes 1179652
  173.9 11.0 %copy-start.3 = (bf16[512,256]{1,0:T(8,128)(2,1)}, bf16[512,256]{1,0:T(8,128)(2,1)S(1)}, u32[]{:S(2)}) copy-start(bf16[512,256]{1,0:T(8,128)(2,1)S(1)} %all-gather.2) | copy-start | bytes 786436
  174.2 11.6 %copy-start.10 = (bf16[6,128,256]{2,1,0:T(8,128)(2,1)}, bf16[6,128,256]{2,1,0:T(8,128)(2,1)S(1)}, u32[]{:S(2)}) copy-start(bf16[6,128,256]{2,1,0:T(8,128)(2,1)S(1)} %fusion.54) | copy-start | bytes 1179652
  184.9 0.9 copy-start.4
  185.8 138.4 %all-gather.12.cloned.1.call-start = ((), (), s32[]{:S(2)}) async-start(), calls=%async_computation.4 | async-start | bytes 1114112 | tf_op jit(solution)/shard_map/all_gather | solution.py:31
  236.9 7.5 %collective-permute-start = (bf16[1,256]{1,0:T(2,128)(2,1)S(1)}, bf16[1,256]{1,0:T(2,128)(2,1)S(1)}, u32[]{:S(2)}, u32[]{:S(2)}) collective-permute-start(bf16[1,256]{1,0:T(2,128)(2,1)S(1)} %get-tuple-element.10), channel_id=1, source_target_pairs={{0,8},{8,16},{16,24},{24,32},{32,40},{40,48},{48,56},{56,64},{64,7... | collective-permute-start | bytes 1544 | tf_op jit(solution)/shard_map/ppermute | solution.py:83
  238.8 5.7 %collective-permute-start.1 = (bf16[1,256]{1,0:T(2,128)(2,1)S(1)}, bf16[1,256]{1,0:T(2,128)(2,1)S(1)}, u32[]{:S(2)}, u32[]{:S(2)}) collective-permute-start(bf16[1,256]{1,0:T(2,128)(2,1)S(1)} %get-tuple-element.11), channel_id=1, source_target_pairs={{8,0},{16,8},{24,16},{32,24},{40,32},{48,40},{56,48},{64,56},{72,6... | collective-permute-start | bytes 1544 | tf_op jit(solution)/shard_map/ppermute | solution.py:86
  241.7 1.9 copy-start.6
  254.1 3.7 copy-start.7
  256.1 68.1 %copy-start.15 = (f32[128]{0:T(128)S(1)}, f32[128]{0:T(128)}, u32[]{:S(2)}) copy-start(f32[128]{0:T(128)} %get-tuple-element.47) | copy-start | bytes 1540
  256.1 68.1 %copy-start.16 = (f32[128]{0:T(128)S(1)}, f32[128]{0:T(128)}, u32[]{:S(2)}) copy-start(f32[128]{0:T(128)} %get-tuple-element.15) | copy-start | bytes 1540
  256.1 68.1 %copy-start.17 = (f32[128]{0:T(128)S(1)}, f32[128]{0:T(128)}, u32[]{:S(2)}) copy-start(f32[128]{0:T(128)} %get-tuple-element.16) | copy-start | bytes 1540
  256.1 68.1 %copy-start.18 = (f32[128]{0:T(128)S(1)}, f32[128]{0:T(128)}, u32[]{:S(2)}) copy-start(f32[128]{0:T(128)} %get-tuple-element.17) | copy-start | bytes 1540
  256.2 68.1 %copy-start.19 = (f32[128]{0:T(128)S(1)}, f32[128]{0:T(128)}, u32[]{:S(2)}) copy-start(f32[128]{0:T(128)} %get-tuple-element.18) | copy-start | bytes 1540
  326.3 1.8 copy-start.2
  326.3 1.8 copy-start.8
  326.3 1.8 copy-start.9
  328.0 3.6 copy-start.14
Sparse Core Ops, SparseCore 0:
  12.4 147.9 all-gather.7
  185.9 68.0 all-gather.9
  256.2 67.9 all-gather.11
where the time goes:
time: 379 us; the launch traced here: 378 us
  waiting for transfers between devices  198 us (52%)
  blocking collectives  101 us (27%)
  matrix products  24 us (6%)
  local copies, waits for them, and re-layouts  15.1 us (4%)
  starting transfers between devices  13.7 us (4%)
  between operations  13.6 us (4%)
  other arithmetic  12.1 us (3%)
    all_gather x1, waiting for transfers between devices, rows_first(): filled = lax.all_gather(both, axis, axis=0, tiled=True)  105 us
    all_gather x2, waiting for transfers between devices, prefix_by_axis(): lax.all_gather(part.astype(kind), axis)  73 us
    all_gather x5, blocking collectives, prefix_by_axis(): lax.all_gather(part.astype(kind), axis)  65.4 us
    all_to_all x1, blocking collectives, sum_at_owner(): lax.all_to_all(blocks, axis, split_axis=0, concat_axis=0, tiled=True)  35.6 us
    all_to_all x1, waiting for transfers between devices, copy_for_each(): lax.all_to_all(jnp.broadcast_to(array[None], (count, *array.shape)), axis...  19.8 us
    dot_general x8, matrix products, project(): return jnp.dot(normed, weight, preferred_element_type=jnp.float32)  14 us
    all_to_all x1, starting transfers between devices, copy_for_each(): lax.all_to_all(jnp.broadcast_to(array[None], (count, *array.shape)), axis...  10.5 us
  transfers between devices with their start and end apart: 6, of which 4 were waited for; matrix products, arithmetic and copies ran while one was open for 8% of the time, Pallas kernels for 0%

commit v1 on v0

v1 whole, which is shorter than its diff:
```python
import functools
import math

import jax
import jax.numpy as jnp
from jax import lax
from jax.experimental import pallas as pl
from jax.experimental.pallas import tpu as pltpu
from jax.sharding import Mesh
from jax.sharding import PartitionSpec as P

NZ, NY, NX, NC = 16, 4, 4, 2
KEY_DIM = 128
VAL_DIM = 256
BLOCK = 64
ROWS = 48
LEN = 384
WIDTH = 2048
EPSILON = 1e-06
SP = ("z", "y")
TP = ("x", "c")
SP_TP = ("z", "y", "x", "c")
F32 = jnp.float32
BF16 = jnp.bfloat16
MESH = pl.DeviceIdType.MESH
N_SEND = 192
N_RECV = 192


def mm(a, b):
    return lax.dot_general(a, b, (((1,), (0,)), ((), ())), preferred_element_type=F32)


def mm_nt(a, b):
    return lax.dot_general(a, b, (((1,), (1,)), ((), ())), preferred_element_type=F32)


def mm_tn(a, b):
    return lax.dot_general(a, b, (((0,), (0,)), ((), ())), preferred_element_type=F32)


def wrap(value, size):
    return lax.rem(value + size, size)


def split3(row):
    hi = row.astype(BF16)
    rest = row - hi.astype(F32)
    mid = rest.astype(BF16)
    low = (rest - mid.astype(F32)).astype(BF16)
    return hi, mid, low


def log_rows(row):
    hi, mid, low = split3(row)
    index = lax.broadcasted_iota(jnp.int32, (16, KEY_DIM), 0)
    spread = [jnp.broadcast_to(p.astype(F32), (16, KEY_DIM)) for p in (hi, mid, low)]
    out = jnp.where(index == 0, spread[0], jnp.where(index == 1, spread[1], jnp.where(index == 2, spread[2], 0.0)))
    return out.astype(BF16)


def log_total(rows16):
    return jnp.sum(rows16.astype(F32), axis=0, keepdims=True)


def kernel(
    tok, norm_gain, wa, wb, taps, ddown, dup, dbias, dextra, hgain,
    out,
    WA, WB, T, SS, R1, M2, R2, M3, IF, IB, CI, CP, HP, HN, XC, PO, PS, PR, XS, XR,
    ssem, rsem,
):
    z, y, x, c = (lax.axis_index(a) for a in SP_TP)
    tp = x * 2 + c
    s = z * 4 + y
    other = 1 - c
    names = {}
    sends = []

    def at(dz=0, dy=0, dx=0, flip=False):
        return (wrap(z + dz, NZ), wrap(y + dy, NY), wrap(x + dx, NX), other if flip else c)

    def sem(name):
        return rsem.at[names.setdefault(name, len(names))]

    def send(src, dst, name, device):
        copy = pltpu.make_async_remote_copy(
            src_ref=src, dst_ref=dst, send_sem=ssem.at[len(sends)], recv_sem=sem(name),
            device_id=device, device_id_type=MESH,
        )
        copy.start()
        sends.append(copy)

    def arrived(dst, name):
        pltpu.make_async_remote_copy(
            src_ref=dst, dst_ref=dst, send_sem=ssem.at[0], recv_sem=sem(name),
            device_id=(z, y, x, c), device_id_type=MESH,
        ).wait_recv()

    after = lax.rem(s + 1, NZ * NY)
    ahead = lax.rem(s + NZ * NY - 1, NZ * NY)
    next_dev = (after // NY, lax.rem(after, NY), x, c)
    prev_dev = (ahead // NY, lax.rem(ahead, NY), x, c)
    peers = [at(dz=d) for d in range(1, NZ)]
    peers += [at(dy=d) for d in range(1, NY)]
    peers += [at(dx=d) for d in range(1, NX)]
    peers += [at(flip=True), next_dev, prev_dev]
    barrier = pltpu.get_barrier_semaphore()
    for peer in peers:
        pl.semaphore_signal(barrier, inc=1, device_id=peer, device_id_type=MESH)

    def token_rows(dx=0, flip=False):
        index = wrap(x + dx, NX) * 2 + (other if flip else c)
        return pl.ds(pl.multiple_of(index * ROWS, 16), ROWS)

    raw_rows = tok[...].astype(F32)
    scale = lax.rsqrt(jnp.mean(raw_rows * raw_rows, axis=-1, keepdims=True) + EPSILON)
    T[token_rows(), :] = (raw_rows * scale * norm_gain[...]).astype(BF16)

    def slot(dz=0, dy=0):
        index = wrap(z + dz, NZ) * NY + wrap(y + dy, NY)
        return pl.ds(pl.multiple_of(index * 32, 32), 32)

    def plane(dz=0):
        return pl.ds(pl.multiple_of(wrap(z + dz, NZ) * 128, 128), 128)

    WA[slot(), :] = wa[...]
    WB[slot(), :] = wb[...]

    pl.semaphore_wait(barrier, len(peers))

    for d in range(1, NY):
        send(wa, WA.at[slot()], ("ay", d), at(dy=d))
    own_rows = T.at[token_rows()]
    send(own_rows, own_rows, "tm", at(dx=1))
    send(own_rows, own_rows, "tp", at(dx=-1))
    send(own_rows, own_rows, ("tc", 0), at(flip=True))
    send(wb, WB.at[slot()], ("zm", 1), at(dz=1))
    send(wb, WB.at[slot()], ("zp", 1), at(dz=-1))
    send(wb, WB.at[slot()], ("ym", 0), at(dy=1))
    send(wb, WB.at[slot()], ("yp", 0), at(dy=-1))

    for d in range(1, NY):
        arrived(WA.at[slot(dy=-d)], ("ay", d))
    send(WA.at[plane()], WA.at[plane()], ("am", 1), at(dz=1))
    send(WA.at[plane()], WA.at[plane()], ("ap", 1), at(dz=-1))

    half = WIDTH // 2

    def token_step(stage):
        if stage == 0:
            ref = T.at[token_rows(dx=-1)]
            arrived(ref, "tm")
            piece = T.at[token_rows(dx=-1), pl.ds(0, half)]
            send(piece, piece, "t2a", at(dx=1))
            send(ref, ref, ("tc", 1), at(flip=True))
            ref = T.at[token_rows(dx=1)]
            arrived(ref, "tp")
            piece = T.at[token_rows(dx=1), pl.ds(half, half)]
            send(piece, piece, "t2b", at(dx=-1))
            send(ref, ref, ("tc", 2), at(flip=True))
        else:
            arrived(T.at[token_rows(dx=2), pl.ds(0, half)], "t2a")
            arrived(T.at[token_rows(dx=2), pl.ds(half, half)], "t2b")
            ref = T.at[token_rows(dx=2)]
            send(ref, ref, ("tc", 3), at(flip=True))

    def place(j):
        return 0 if j == 0 else (-j if j <= 8 else j - 8)

    def plus(j):
        return (j % 2 == 0) if j <= 8 else ((j - 8) % 2 == 1)

    def column_step(j):
        dz = place(j)
        ref = WB.at[slot(dz, -1)]
        arrived(ref, ("ym", j))
        if plus(j):
            send(ref, ref, ("y2", j), at(dy=1))
        ref = WB.at[slot(dz, 1)]
        arrived(ref, ("yp", j))
        if not plus(j):
            send(ref, ref, ("y2", j), at(dy=-1))

    def fan_out(j):
        ref = WB.at[slot(place(j))]
        send(ref, ref, ("ym", j), at(dy=1))
        send(ref, ref, ("yp", j), at(dy=-1))

    for k in range(1, 9):
        ref = WA.at[plane(-k)]
        arrived(ref, ("am", k))
        if k < 8:
            send(ref, ref, ("am", k + 1), at(dz=1))
            ref = WA.at[plane(k)]
            arrived(ref, ("ap", k))
            if k < 7:
                send(ref, ref, ("ap", k + 1), at(dz=-1))
        ref = WB.at[slot(-k)]
        arrived(ref, ("zm", k))
        if k < 8:
            send(ref, ref, ("zm", k + 1), at(dz=1))
        fan_out(k)
        if k < 8:
            ref = WB.at[slot(k)]
            arrived(ref, ("zp", k))
            if k < 7:
                send(ref, ref, ("zp", k + 1), at(dz=-1))
            fan_out(8 + k)
        if k == 2:
            token_step(0)
        if k == 4:
            token_step(1)
        column_step(k - 1)
        if k > 1:
            column_step(7 + k)
    column_step(8)
    for j in range(4):
        arrived(T.at[token_rows(dx=(0, -1, 1, 2)[j], flip=True)], ("tc", j))
    for j in range(16):
        arrived(WB.at[slot(place(j), 2)], ("y2", j))

    normed = T[...]
    kv = mm(normed, WA[...])
    key_f = kv[:, :KEY_DIM].astype(BF16).astype(F32)
    value = kv[:, KEY_DIM:].astype(BF16)
    low = mm(normed, ddown[...]).astype(BF16)
    key_cols = pl.ds(pl.multiple_of(tp * KEY_DIM, KEY_DIM), KEY_DIM)
    val_cols = pl.ds(pl.multiple_of(tp * VAL_DIM, VAL_DIM), VAL_DIM)
    pre = mm(low, dup[:, key_cols]) + dbias[:, key_cols]
    log_sig = jnp.minimum(pre, 0.0) - jnp.log1p(jnp.exp(-jnp.abs(pre)))
    extra = jnp.transpose(jnp.broadcast_to(dextra[...], (KEY_DIM, LEN)))
    log_decay = log_sig / 16.0 + extra
    ri = lax.broadcasted_iota(jnp.int32, (LEN, LEN), 0)
    ci = lax.broadcasted_iota(jnp.int32, (LEN, LEN), 1)
    tri = jnp.where((ri >= ci) & (ri // BLOCK == ci // BLOCK), 1.0, 0.0).astype(F32)
    cumul = lax.dot_general(
        tri, log_decay, (((1,), (0,)), ((), ())), precision=lax.Precision.HIGHEST, preferred_element_type=F32
    )
    before = cumul - log_decay
    blocks = LEN // BLOCK

    def part(array, n):
        return array[n * BLOCK : (n + 1) * BLOCK]

    totals = [cumul[(n + 1) * BLOCK - 1 : (n + 1) * BLOCK] for n in range(blocks)]
    offsets = [jnp.zeros((1, KEY_DIM), F32)]
    for n in range(blocks):
        offsets.append(offsets[-1] + totals[n])
    whole = offsets[blocks]
    suffix = [jnp.zeros((1, KEY_DIM), F32)]
    for n in reversed(range(blocks)):
        suffix.append(suffix[-1] + totals[n])
    suffix = suffix[::-1][1:]
    to_end = jnp.concatenate([suffix[n] + totals[n] - part(cumul, n) for n in range(blocks)], axis=0)
    from_start = jnp.concatenate([offsets[n] + part(before, n) for n in range(blocks)], axis=0)
    fwd_device = mm_tn(value, (key_f * jnp.exp(to_end)).astype(BF16))
    back_device = mm_tn(value, (key_f * jnp.exp(from_start)).astype(BF16))

    marks = log_rows(whole)
    for q in range(NY):
        SS[q * 144 : q * 144 + 64, :] = fwd_device[q * 64 : q * 64 + 64].astype(BF16)
        SS[q * 144 + 64 : q * 144 + 128, :] = back_device[q * 64 : q * 64 + 64].astype(BF16)
        SS[q * 144 + 128 : q * 144 + 144, :] = marks

    def message(dy=0):
        return pl.ds(pl.multiple_of(wrap(y + dy, NY) * 144, 16), 144)

    R1[message(), :] = SS[message(), :]
    for d in range(1, NY):
        send(SS.at[message(d)], R1.at[message()], ("s1", d), at(dy=d))

    qcg = mm(normed, WB[:, 0:640])
    query_f = (qcg[:, :KEY_DIM] * (1.0 / math.sqrt(KEY_DIM))).astype(BF16).astype(F32)
    conv_in = qcg[:, KEY_DIM : KEY_DIM + 256].astype(BF16)
    gate = qcg[:, KEY_DIM + 256 :].astype(BF16).astype(F32)
    CI[...] = conv_in
    CP[8 : 8 + LEN, :] = conv_in.astype(F32)
    send(CI.at[pl.ds(LEN - 16, 16)], HP, "hp", next_dev)
    send(CI.at[pl.ds(0, 16)], HN, "hn", prev_dev)

    for d in range(1, NY):
        arrived(R1.at[message(-d)], ("s1", d))
    in_f, in_b, in_l = [], [], []
    for q in range(NY):
        in_f.append(R1[q * 144 : q * 144 + 64, :].astype(F32))
        in_b.append(R1[q * 144 + 64 : q * 144 + 128, :].astype(F32))
        in_l.append(log_total(R1[q * 144 + 128 : q * 144 + 144, :]))
    total_f = jnp.zeros((64, KEY_DIM), F32)
    total_b = jnp.zeros((64, KEY_DIM), F32)
    log_f = jnp.zeros((1, KEY_DIM), F32)
    log_b = jnp.zeros((1, KEY_DIM), F32)
    plane_f, plane_b, gap_f, gap_b = ([None] * NY for _ in range(4))
    for q in range(NY):
        plane_f[q], gap_f[q] = total_f, log_f
        total_f = jnp.exp(in_l[q]) * total_f + in_f[q]
        log_f = log_f + in_l[q]
    for q in reversed(range(NY)):
        plane_b[q], gap_b[q] = total_b, log_b
        total_b = jnp.exp(in_l[q]) * total_b + in_b[q]
        log_b = log_b + in_l[q]
    marks = log_rows(log_f)
    M2[0:64, :] = total_f.astype(BF16)
    M2[64:80, :] = marks
    M2[80:144, :] = total_b.astype(BF16)
    M2[144:160, :] = marks

    def depth(dz=0):
        return pl.ds(pl.multiple_of(wrap(z + dz, NZ) * 80, 16), 80)

    R2[depth(), :] = M2[0:80, :]
    for d in (8, 7, 9, 6, 10, 5, 11, 4, 12, 3, 13, 2, 14, 1, 15):
        start = pl.multiple_of(((z + d) // NZ) * 80, 16)
        send(M2.at[pl.ds(start, 80)], R2.at[depth()], ("s2", d), at(dz=d))

    lower = lax.broadcasted_iota(jnp.int32, (BLOCK, BLOCK), 0) >= lax.broadcasted_iota(jnp.int32, (BLOCK, BLOCK), 1)
    upper = lax.broadcasted_iota(jnp.int32, (BLOCK, BLOCK), 0) <= lax.broadcasted_iota(jnp.int32, (BLOCK, BLOCK), 1)
    within = []
    fwd_inc, back_inc, fwd_query, back_query = [], [], [], []
    for n in range(blocks):
        cum_n, bef_n, key_n, query_n, value_n = (part(a, n) for a in (cumul, before, key_f, query_f, value))
        fq = (query_n * jnp.exp(cum_n)).astype(BF16)
        ks = (key_n * jnp.exp(bef_n)).astype(BF16)
        fwd_scores = mm_nt(fq, (key_n * jnp.exp(-cum_n)).astype(BF16))
        back_scores = mm_nt((query_n * jnp.exp(-bef_n)).astype(BF16), ks)
        scores = jnp.where(lower, fwd_scores, 0.0) + jnp.where(upper, back_scores, 0.0)
        within.append(mm(scores.astype(BF16), value_n))
        fwd_inc.append(mm_tn(value_n, (key_n * jnp.exp(totals[n] - cum_n)).astype(BF16)))
        back_inc.append(mm_tn(value_n, ks))
        fwd_query.append(fq)
        back_query.append((query_n * jnp.exp(totals[n] - bef_n)).astype(BF16))
    state = fwd_inc[0]
    for n in range(1, blocks):
        within[n] = within[n] + mm_nt(fwd_query[n], state.astype(BF16))
        state = jnp.exp(totals[n]) * state + fwd_inc[n]
    state = back_inc[blocks - 1]
    for n in reversed(range(blocks - 1)):
        within[n] = within[n] + mm_nt(back_query[n], state.astype(BF16))
        state = jnp.exp(totals[n]) * state + back_inc[n]
    local = jnp.concatenate(within, axis=0)
    far_fwd = jnp.concatenate(
        [part(query_f, n) * jnp.exp(offsets[n] + part(cumul, n)) for n in range(blocks)], axis=0
    ).astype(BF16)
    far_back = jnp.concatenate(
        [part(query_f, n) * jnp.exp(suffix[n] + (totals[n] - part(before, n))) for n in range(blocks)], axis=0
    ).astype(BF16)

    arrived(HP, "hp")
    arrived(HN, "hn")
    first = HP[...].astype(F32)[15:16]
    last = HN[...].astype(F32)[0:1]
    CP[7:8, :] = jnp.where(s > 0, first, 0.0)
    CP[8 + LEN : 9 + LEN, :] = jnp.where(s < NZ * NY - 1, last, 0.0)
    tap = taps[:, val_cols]
    mixed = CP[7 : 7 + LEN, :] * tap[0:1] + CP[8 : 8 + LEN, :] * tap[1:2] + CP[9 : 9 + LEN, :] * tap[2:3]
    XC[:, 0:256] = (mixed * (gate * (1.0 / (1.0 + jnp.exp(-gate))))).astype(BF16)

    for d in range(1, NZ):
        arrived(R2.at[depth(-d)], ("s2", d))
    sum_f = jnp.zeros((64, KEY_DIM), F32)
    sum_b = jnp.zeros((64, KEY_DIM), F32)
    for k in range(NZ):
        step = jnp.exp(log_total(R2[k * 80 + 64 : k * 80 + 80, :])) * sum_f + R2[k * 80 : k * 80 + 64, :].astype(F32)
        sum_f = jnp.where(k < z, step, sum_f)
    for k in reversed(range(NZ)):
        step = jnp.exp(log_total(R2[k * 80 + 64 : k * 80 + 80, :])) * sum_b + R2[k * 80 : k * 80 + 64, :].astype(F32)
        sum_b = jnp.where(k > z, step, sum_b)
    for q in range(NY):
        M3[q * 128 : q * 128 + 64, :] = (plane_f[q] + jnp.exp(gap_f[q]) * sum_f).astype(BF16)
        M3[q * 128 + 64 : q * 128 + 128, :] = (plane_b[q] + jnp.exp(gap_b[q]) * sum_b).astype(BF16)

    def quarter(dy=0):
        return pl.ds(pl.multiple_of(wrap(y + dy, NY) * 64, 64), 64)

    def answer(dy, which):
        return pl.ds(pl.multiple_of(wrap(y + dy, NY) * 128 + 64 * which, 64), 64)

    for d in range(1, NY):
        send(M3.at[answer(d, 0)], IF.at[quarter()], ("s3f", d), at(dy=d))
        send(M3.at[answer(d, 1)], IB.at[quarter()], ("s3b", d), at(dy=d))
    IF[quarter(), :] = M3[answer(0, 0), :]
    IB[quarter(), :] = M3[answer(0, 1), :]
    for d in range(1, NY):
        arrived(IF.at[quarter(-d)], ("s3f", d))
        arrived(IB.at[quarter(-d)], ("s3b", d))
    raw = local + mm_nt(far_fwd, IF[...]) + mm_nt(far_back, IB[...])
    norm = lax.rsqrt(jnp.mean(raw * raw, axis=-1, keepdims=True) + EPSILON)
    XC[:, 256:512] = (raw * norm * hgain[:, val_cols]).astype(BF16)

    def block4(r):
        return pl.ds(r * ROWS, ROWS)

    order = (2, 1, 3, 0)
    there = jnp.concatenate([XC[token_rows(dx=r, flip=True), :] for r in order], axis=0)
    here = jnp.concatenate([XC[token_rows(dx=r), :] for r in order], axis=0)
    for n in range(0, WIDTH, 512):
        PS[:, n : n + 512] = mm_nt(there, WB[n : n + 512, 640:1152]).astype(BF16)
    for i in range(4):
        send(PS.at[block4(i)], PR.at[block4(i)], ("pr", i), at(flip=True))
    for n in range(0, WIDTH, 512):
        PO[:, n : n + 512] = mm_nt(here, WB[n : n + 512, 640:1152])
    for i in range(3):
        arrived(PR.at[block4(i)], ("pr", i))
        XS[i * ROWS : (i + 1) * ROWS, :] = (
            PO[i * ROWS : (i + 1) * ROWS, :] + PR[i * ROWS : (i + 1) * ROWS, :].astype(F32)
        ).astype(BF16)
        send(XS.at[block4(i)], XR.at[block4(i)], ("xr", i), at(dx=order[i]))
    arrived(PR.at[block4(3)], ("pr", 3))
    total = PO[3 * ROWS :, :] + PR[3 * ROWS :, :].astype(F32)
    for i in (1, 2, 0):
        arrived(XR.at[block4(i)], ("xr", i))
        total = total + XR[i * ROWS : (i + 1) * ROWS, :].astype(F32)
    out[...] = total.astype(BF16)

    for copy in sends:
        copy.wait_send()
    assert len(sends) <= N_SEND and len(names) <= N_RECV, (len(sends), len(names))


def local(
    tokens, norm_gain, conv_in_weight, conv_gate_weight, conv_taps, query_weight, key_weight, value_weight,
    decay_down, decay_up, decay_bias, decay_extra, head_gain, conv_out_weight, value_out_weight,
):
    wa = jnp.concatenate([key_weight, value_weight], axis=1)
    wb = jnp.concatenate(
        [query_weight, conv_in_weight, conv_gate_weight, conv_out_weight.T, value_out_weight.T], axis=1
    )
    vmem = pl.BlockSpec(memory_space=pltpu.VMEM)
    return pl.pallas_call(
        kernel,
        out_shape=jax.ShapeDtypeStruct((ROWS, WIDTH), BF16),
        in_specs=[vmem] * 10,
        out_specs=vmem,
        scratch_shapes=[
            pltpu.VMEM((2048, 384), BF16),
            pltpu.VMEM((2048, 1152), BF16),
            pltpu.VMEM((LEN, WIDTH), BF16),
            pltpu.VMEM((NY * 144, KEY_DIM), BF16),
            pltpu.VMEM((NY * 144, KEY_DIM), BF16),
            pltpu.VMEM((160, KEY_DIM), BF16),
            pltpu.VMEM((NZ * 80, KEY_DIM), BF16),
            pltpu.VMEM((NY * 128, KEY_DIM), BF16),
            pltpu.VMEM((VAL_DIM, KEY_DIM), BF16),
            pltpu.VMEM((VAL_DIM, KEY_DIM), BF16),
            pltpu.VMEM((LEN, 256), BF16),
            pltpu.VMEM((LEN + 16, 256), F32),
            pltpu.VMEM((16, 256), BF16),
            pltpu.VMEM((16, 256), BF16),
            pltpu.VMEM((LEN, 512), BF16),
            pltpu.VMEM((4 * ROWS, WIDTH), F32),
            pltpu.VMEM((4 * ROWS, WIDTH), BF16),
            pltpu.VMEM((4 * ROWS, WIDTH), BF16),
            pltpu.VMEM((3 * ROWS, WIDTH), BF16),
            pltpu.VMEM((3 * ROWS, WIDTH), BF16),
            pltpu.SemaphoreType.DMA((N_SEND,)),
            pltpu.SemaphoreType.DMA((N_RECV,)),
        ],
        compiler_params=pltpu.CompilerParams(collective_id=0, has_side_effects=True, vmem_limit_bytes=60 * 1024 * 1024),
        cost_estimate=pl.CostEstimate(flops=3_000_000_000, bytes_accessed=1_000_000, transcendentals=0),
    )(
        tokens, norm_gain.reshape(1, -1), wa, wb, conv_taps, decay_down, decay_up,
        decay_bias.reshape(1, -1), decay_extra, head_gain.reshape(1, -1),
    )


def solution(mesh):
    torus = Mesh(mesh.devices.reshape(NZ, NY, NX, NC), SP_TP)
    return jax.shard_map(
        local,
        mesh=torus,
        in_specs=(
            P(SP_TP, None), P(), P(SP, TP), P(SP, TP), P(), P(SP, TP), P(SP, TP), P(SP, TP),
            P(), P(), P(), P(TP, SP), P(), P(TP, SP), P(TP, SP),
        ),
        out_specs=P(SP_TP, None),
        check_vma=False,
    )
```

time: 379 us -> 116 us (0.31)
  waiting for transfers between devices: 198 us -> 0 us
  Pallas kernels: 0 us -> 110 us
  blocking collectives: 101 us -> 0 us
  matrix products: 24 us -> 0 us
  starting transfers between devices: 13.7 us -> 0 us
  between operations: 13.6 us -> 0.04 us
  local copies, waits for them, and re-layouts: 15.1 us -> 4.16 us
  other arithmetic: 12.1 us -> 1.35 us
    all_gather x3 -> x0, waiting for transfers between devices: 178 us -> none  [the longest x1 105 us: rows_first(): filled = lax.all_gather(both, axis, axis=0, tiled=True)]
    pallas_call x0 -> x1, Pallas kernels: none -> 110 us  [local(): pl.pallas_call(kernel, out_shape=jax.ShapeDtypeStruct((ROWS, WIDTH), BF16...]
    all_gather x5 -> x0, blocking collectives: 65.4 us -> none  [prefix_by_axis(): lax.all_gather(part.astype(kind), axis)]
    all_to_all x1 -> x0, blocking collectives: 35.6 us -> none  [sum_at_owner(): lax.all_to_all(blocks, axis, split_axis=0, concat_axis=0, tiled=True)]
    dot_general x18 -> x0, matrix products: 24 us -> none  [the longest x8 14 us: project(): return jnp.dot(normed, weight, preferred_element_type=jnp.float32)]
    all_to_all x1 -> x0, waiting for transfers between devices: 19.8 us -> none  [copy_for_each(): lax.all_to_all(jnp.broadcast_to(array[None], (count, *array.shape)), axis...]
    all_to_all x1 -> x0, starting transfers between devices: 10.5 us -> none  [copy_for_each(): lax.all_to_all(jnp.broadcast_to(array[None], (count, *array.shape)), axis...]
    mul x4 -> x0, other arithmetic: 5.15 us -> none  [the longest x1 2.03 us: gla_heads(): tail_decay[..., None] * incoming_back[None]]
  transfers between devices with their start and end apart: 6 -> 0, of which waited for: 4 -> 0; matrix products, arithmetic and copies ran while one was open for 8% -> 0% of each run, Pallas kernels for 0% -> 0%
where the time goes in v1:
time: 116 us
  Pallas kernels  110 us (95%)
  local copies, waits for them, and re-layouts  4.16 us (4%)
  other arithmetic  1.35 us (1%)
    pallas_call x1, Pallas kernels, local(): pl.pallas_call(kernel, out_shape=jax.ShapeDtypeStruct((ROWS, WIDTH), BF16...  110 us
    unnamed x20, local copies, waits for them, and re-layouts  4.16 us

profile of v1, /device:TPU:1, one launch (start us, length us, event | category | flops | bytes accessed | tf_op | source)
XLA Modules:
  0.0 115.5 jit_solution(9679403962559660395)
XLA Ops:
  0.0 0.0 copy-start.5
  0.0 1.3 %pad_maximum_fusion.wa = bf16[32,384]{1,0:T(8,128)(2,1)} fusion(bf16[32,256]{1,0:T(8,128)(2,1)} %param.22, bf16[32,128]{1,0:T(8,128)(2,1)} %param.21), kind=kLoop, calls=%fused_computation | loop fusion | flops 49152 | bytes 49152 | tf_op jit(solution)/shard_map/concatenate | solution.py:423
  1.4 0.0 copy-done.5
  1.4 0.0 copy-start.1
  1.4 0.0 copy-start.2
  1.4 0.0 copy-start.3
  1.4 0.0 copy-start.4
  1.4 0.7 copy-done.1
  2.1 0.0 copy-start
  2.1 0.0 copy-done.2
  2.1 0.0 copy-done.3
  2.1 0.0 copy-done.4
  2.1 0.8 copy-done
  2.9 0.0 copy-start.6
  2.9 1.0 copy.16.ddown
  3.9 0.0 copy-done.6
  3.9 110.0 %shard_map.145 = bf16[48,2048]{1,0:T(8,128)(2,1)} custom-call(bf16[48,2048]{1,0:T(8,128)(2,1)} %tok.1, f32[1,2048]{1,0:T(1,128)} %bitcast.7, bf16[32,384]{1,0:T(8,128)(2,1)} %pad_maximum_fusion.wa, bf16[32,1152]{1,0:T(8,128)(2,1)} %copy-done.6, f32[3,2048]{1,0:T(4,128)} %taps.1, bf16[2048,16]{1,0:T(8,128)(2,1)} %copy.16.ddown, bf16[16,1024]{1,0:T(8,128)(2,1)} %dup.1, ...), custom_call_target="tpu_custom_call" | custom-call | flops 3000000000 | bytes 1000000 | tf_op jit(solution)/shard_map/pallas_call | solution.py:428
  113.9 1.6 %copy.22 = bf16[48,2048]{1,0:T(8,128)(2,1)} copy(bf16[48,2048]{1,0:T(8,128)(2,1)} %shard_map.145) | data formatting | bytes 393216
  (5 shorter events, 0.0 us)
Async XLA Ops:
  0.0 1.4 %copy-start.5 = (bf16[32,128]{1,0:T(8,128)(2,1)S(1)}, bf16[32,128]{1,0:T(8,128)(2,1)}, u32[]{:S(2)}) copy-start(bf16[32,128]{1,0:T(8,128)(2,1)} %param.20) | copy-start | bytes 24580
  1.4 0.7 copy-start.1
  1.4 0.7 copy-start.2
  1.4 0.7 copy-start.3
  1.4 0.8 copy-start.4
  2.1 0.8 copy-start
  2.9 1.0 copy-start.6

commit v2 on v1

--- a/solution.py
+++ b/solution.py
@@ -23,8 +23,8 @@
 F32 = jnp.float32
 BF16 = jnp.bfloat16
 MESH = pl.DeviceIdType.MESH
-N_SEND = 192
-N_RECV = 192
+N_SEND = 256
+N_RECV = 256
 
 
 def mm(a, b):
@@ -64,10 +64,11 @@
 
 
 def kernel(
-    tok, norm_gain, wa, wb, taps, ddown, dup, dbias, dextra, hgain,
+    tok_h, gain_h, ci_h, cg_h, taps_h, q_h, k_h, v_h, dd_h, du_h, db_h, de_h, hg_h, co_h, vo_h,
     out,
-    WA, WB, T, SS, R1, M2, R2, M3, IF, IB, CI, CP, HP, HN, XC, PO, PS, PR, XS, XR,
-    ssem, rsem,
+    tok, norm_gain, taps, ddown, dup, dbias, dextra, hgain,
+    WA, WB, WC, T, SS, R1, M2, R2, M3, IF, IB, CI, CP, HP, HN, XC, PO, PS, PR, XS, XR,
+    ssem, rsem, lsem,
 ):
     z, y, x, c = (lax.axis_index(a) for a in SP_TP)
     tp = x * 2 + c
@@ -100,7 +101,7 @@
     ahead = lax.rem(s + NZ * NY - 1, NZ * NY)
     next_dev = (after // NY, lax.rem(after, NY), x, c)
     prev_dev = (ahead // NY, lax.rem(ahead, NY), x, c)
-    peers = [at(dz=d) for d in range(1, NZ)]
+    peers = [at(dz=d) for d in (1, -1)]
     peers += [at(dy=d) for d in range(1, NY)]
     peers += [at(dx=d) for d in range(1, NX)]
     peers += [at(flip=True), next_dev, prev_dev]
@@ -108,43 +109,121 @@
     for peer in peers:
         pl.semaphore_signal(barrier, inc=1, device_id=peer, device_id_type=MESH)
 
+    def slot(dz=0, dy=0):
+        index = wrap(z + dz, NZ) * NY + wrap(y + dy, NY)
+        return pl.ds(pl.multiple_of(index * 32, 32), 32)
+
+    def plane(dz=0):
+        return pl.ds(pl.multiple_of(wrap(z + dz, NZ) * 128, 128), 128)
+
     def token_rows(dx=0, flip=False):
         index = wrap(x + dx, NX) * 2 + (other if flip else c)
         return pl.ds(pl.multiple_of(index * ROWS, 16), ROWS)
 
+    loads = []
+
+    def load(src, dst):
+        copy = pltpu.make_async_copy(src, dst, lsem.at[len(loads)])
+        copy.start()
+        loads.append(copy)
+
+    load(k_h, WA.at[slot(), pl.ds(0, 128)])
+    load(v_h, WA.at[slot(), pl.ds(128, 256)])
+    load(tok_h, tok)
+    load(gain_h, norm_gain)
+    load(q_h, WB.at[slot(), pl.ds(0, 128)])
+    load(ci_h, WB.at[slot(), pl.ds(128, 256)])
+    load(cg_h, WB.at[slot(), pl.ds(384, 256)])
+    load(co_h, WC.at[slot(), pl.ds(0, 256)])
+    load(vo_h, WC.at[slot(), pl.ds(256, 256)])
+    load(dd_h, ddown)
+    load(du_h, dup)
+    load(db_h, dbias)
+    load(de_h, dextra)
+    load(taps_h, taps)
+    load(hg_h, hgain)
+    for copy in loads[:4]:
+        copy.wait()
     raw_rows = tok[...].astype(F32)
     scale = lax.rsqrt(jnp.mean(raw_rows * raw_rows, axis=-1, keepdims=True) + EPSILON)
     T[token_rows(), :] = (raw_rows * scale * norm_gain[...]).astype(BF16)
-
-    def slot(dz=0, dy=0):
-        index = wrap(z + dz, NZ) * NY + wrap(y + dy, NY)
-        return pl.ds(pl.multiple_of(index * 32, 32), 32)
-
-    def plane(dz=0):
-        return pl.ds(pl.multiple_of(wrap(z + dz, NZ) * 128, 128), 128)
-
-    WA[slot(), :] = wa[...]
-    WB[slot(), :] = wb[...]
+    for copy in loads[4:]:
+        copy.wait()
 
     pl.semaphore_wait(barrier, len(peers))
 
+    def place(j):
+        return 0 if j == 0 else (-j if j <= 8 else j - 8)
+
+    def plus(j):
+        return (j % 2 == 0) if j <= 8 else ((j - 8) % 2 == 1)
+
+    class Ring:
+        def __init__(self, W, tag):
+            self.W, self.tag = W, tag
+
+        def around(self):
+            ref = self.W.at[slot()]
+            send(ref, ref, (self.tag, "zm", 1), at(dz=1))
+            send(ref, ref, (self.tag, "zp", 1), at(dz=-1))
+
+        def fan_out(self, j):
+            ref = self.W.at[slot(place(j))]
+            send(ref, ref, (self.tag, "ym", j), at(dy=1))
+            send(ref, ref, (self.tag, "yp", j), at(dy=-1))
+
+        def step(self, k):
+            ref = self.W.at[slot(-k)]
+            arrived(ref, (self.tag, "zm", k))
+            if k < 8:
+                send(ref, ref, (self.tag, "zm", k + 1), at(dz=1))
+            self.fan_out(k)
+            if k < 8:
+                ref = self.W.at[slot(k)]
+                arrived(ref, (self.tag, "zp", k))
+                if k < 7:
+                    send(ref, ref, (self.tag, "zp", k + 1), at(dz=-1))
+                self.fan_out(8 + k)
+
+        def column(self, j):
+            dz = place(j)
+            ref = self.W.at[slot(dz, -1)]
+            arrived(ref, (self.tag, "ym", j))
+            if plus(j):
+                send(ref, ref, (self.tag, "y2", j), at(dy=1))
+            ref = self.W.at[slot(dz, 1)]
+            arrived(ref, (self.tag, "yp", j))
+            if not plus(j):
+                send(ref, ref, (self.tag, "y2", j), at(dy=-1))
+
+        def columns(self, k):
+            self.column(k - 1)
+            if k > 1:
+                self.column(7 + k)
+
+        def finish(self):
+            for j in range(16):
+                arrived(self.W.at[slot(place(j), 2)], (self.tag, "y2", j))
+
+    ring_b, ring_c = Ring(WB, "b"), Ring(WC, "c")
+    own_a = WA.at[slot()]
     for d in range(1, NY):
-        send(wa, WA.at[slot()], ("ay", d), at(dy=d))
+        send(own_a, own_a, ("ay", d), at(dy=d))
     own_rows = T.at[token_rows()]
     send(own_rows, own_rows, "tm", at(dx=1))
     send(own_rows, own_rows, "tp", at(dx=-1))
     send(own_rows, own_rows, ("tc", 0), at(flip=True))
-    send(wb, WB.at[slot()], ("zm", 1), at(dz=1))
-    send(wb, WB.at[slot()], ("zp", 1), at(dz=-1))
-    send(wb, WB.at[slot()], ("ym", 0), at(dy=1))
-    send(wb, WB.at[slot()], ("yp", 0), at(dy=-1))
-
+    ring_b.around()
+    ring_b.fan_out(0)
     for d in range(1, NY):
         arrived(WA.at[slot(dy=-d)], ("ay", d))
     send(WA.at[plane()], WA.at[plane()], ("am", 1), at(dz=1))
     send(WA.at[plane()], WA.at[plane()], ("ap", 1), at(dz=-1))
 
     half = WIDTH // 2
+    blocks = LEN // BLOCK
+    key_cols = pl.ds(pl.multiple_of(tp * KEY_DIM, KEY_DIM), KEY_DIM)
+    val_cols = pl.ds(pl.multiple_of(tp * VAL_DIM, VAL_DIM), VAL_DIM)
 
     def token_step(stage):
         if stage == 0:
@@ -158,33 +237,31 @@
             piece = T.at[token_rows(dx=1), pl.ds(half, half)]
             send(piece, piece, "t2b", at(dx=-1))
             send(ref, ref, ("tc", 2), at(flip=True))
-        else:
+        elif stage == 1:
             arrived(T.at[token_rows(dx=2), pl.ds(0, half)], "t2a")
             arrived(T.at[token_rows(dx=2), pl.ds(half, half)], "t2b")
             ref = T.at[token_rows(dx=2)]
             send(ref, ref, ("tc", 3), at(flip=True))
-
-    def place(j):
-        return 0 if j == 0 else (-j if j <= 8 else j - 8)
-
-    def plus(j):
-        return (j % 2 == 0) if j <= 8 else ((j - 8) % 2 == 1)
-
-    def column_step(j):
-        dz = place(j)
-        ref = WB.at[slot(dz, -1)]
-        arrived(ref, ("ym", j))
-        if plus(j):
-            send(ref, ref, ("y2", j), at(dy=1))
-        ref = WB.at[slot(dz, 1)]
-        arrived(ref, ("yp", j))
-        if not plus(j):
-            send(ref, ref, ("y2", j), at(dy=-1))
-
-    def fan_out(j):
-        ref = WB.at[slot(place(j))]
-        send(ref, ref, ("ym", j), at(dy=1))
-        send(ref, ref, ("yp", j), at(dy=-1))
+        else:
+            for j in range(4):
+                arrived(T.at[token_rows(dx=(0, -1, 1, 2)[j], flip=True)], ("tc", j))
+
+    def part(array, n):
+        return array[n * BLOCK : (n + 1) * BLOCK]
+
+    def decay():
+        low = mm_nt(T[...], ddown[...]).astype(BF16)
+        pre = mm(low, dup[:, key_cols]) + dbias[:, key_cols]
+        log_sig = jnp.minimum(pre, 0.0) - jnp.log1p(jnp.exp(-jnp.abs(pre)))
+        extra = jnp.transpose(jnp.broadcast_to(dextra[...], (KEY_DIM, LEN)))
+        log_decay = log_sig / 16.0 + extra
+        ri = lax.broadcasted_iota(jnp.int32, (LEN, LEN), 0)
+        ci = lax.broadcasted_iota(jnp.int32, (LEN, LEN), 1)
+        tri = jnp.where((ri >= ci) & (ri // BLOCK == ci // BLOCK), 1.0, 0.0).astype(F32)
+        cumul = lax.dot_general(
+            tri, log_decay, (((1,), (0,)), ((), ())), precision=lax.Precision.HIGHEST, preferred_element_type=F32
+        )
+        return cumul, cumul - log_decay
 
     for k in range(1, 9):
         ref = WA.at[plane(-k)]
@@ -195,68 +272,40 @@
             arrived(ref, ("ap", k))
             if k < 7:
                 send(ref, ref, ("ap", k + 1), at(dz=-1))
-        ref = WB.at[slot(-k)]
-        arrived(ref, ("zm", k))
         if k < 8:
-            send(ref, ref, ("zm", k + 1), at(dz=1))
-        fan_out(k)
-        if k < 8:
-            ref = WB.at[slot(k)]
-            arrived(ref, ("zp", k))
-            if k < 7:
-                send(ref, ref, ("zp", k + 1), at(dz=-1))
-            fan_out(8 + k)
+            ring_b.step(k)
         if k == 2:
             token_step(0)
         if k == 4:
             token_step(1)
-        column_step(k - 1)
-        if k > 1:
-            column_step(7 + k)
-    column_step(8)
-    for j in range(4):
-        arrived(T.at[token_rows(dx=(0, -1, 1, 2)[j], flip=True)], ("tc", j))
-    for j in range(16):
-        arrived(WB.at[slot(place(j), 2)], ("y2", j))
+        if k < 8:
+            ring_b.columns(k)
+        if k == 6:
+            token_step(2)
+            cumul, before = decay()
+            totals = [cumul[(n + 1) * BLOCK - 1 : (n + 1) * BLOCK] for n in range(blocks)]
+            offsets = [jnp.zeros((1, KEY_DIM), F32)]
+            for n in range(blocks):
+                offsets.append(offsets[-1] + totals[n])
+            whole = offsets[blocks]
+            suffix = [jnp.zeros((1, KEY_DIM), F32)]
+            for n in reversed(range(blocks)):
+                suffix.append(suffix[-1] + totals[n])
+            suffix = suffix[::-1][1:]
+            to_end = jnp.concatenate([suffix[n] + totals[n] - part(cumul, n) for n in range(blocks)], axis=0)
+            from_start = jnp.concatenate([offsets[n] + part(before, n) for n in range(blocks)], axis=0)
+            to_end, from_start = jnp.exp(to_end), jnp.exp(from_start)
+            marks = log_rows(whole)
+        if k == 7:
+            ring_c.around()
 
     normed = T[...]
     kv = mm(normed, WA[...])
     key_f = kv[:, :KEY_DIM].astype(BF16).astype(F32)
     value = kv[:, KEY_DIM:].astype(BF16)
-    low = mm(normed, ddown[...]).astype(BF16)
-    key_cols = pl.ds(pl.multiple_of(tp * KEY_DIM, KEY_DIM), KEY_DIM)
-    val_cols = pl.ds(pl.multiple_of(tp * VAL_DIM, VAL_DIM), VAL_DIM)
-    pre = mm(low, dup[:, key_cols]) + dbias[:, key_cols]
-    log_sig = jnp.minimum(pre, 0.0) - jnp.log1p(jnp.exp(-jnp.abs(pre)))
-    extra = jnp.transpose(jnp.broadcast_to(dextra[...], (KEY_DIM, LEN)))
-    log_decay = log_sig / 16.0 + extra
-    ri = lax.broadcasted_iota(jnp.int32, (LEN, LEN), 0)
-    ci = lax.broadcasted_iota(jnp.int32, (LEN, LEN), 1)
-    tri = jnp.where((ri >= ci) & (ri // BLOCK == ci // BLOCK), 1.0, 0.0).astype(F32)
-    cumul = lax.dot_general(
-        tri, log_decay, (((1,), (0,)), ((), ())), precision=lax.Precision.HIGHEST, preferred_element_type=F32
-    )
-    before = cumul - log_decay
-    blocks = LEN // BLOCK
-
-    def part(array, n):
-        return array[n * BLOCK : (n + 1) * BLOCK]
-
-    totals = [cumul[(n + 1) * BLOCK - 1 : (n + 1) * BLOCK] for n in range(blocks)]
-    offsets = [jnp.zeros((1, KEY_DIM), F32)]
-    for n in range(blocks):
-        offsets.append(offsets[-1] + totals[n])
-    whole = offsets[blocks]
-    suffix = [jnp.zeros((1, KEY_DIM), F32)]
-    for n in reversed(range(blocks)):
-        suffix.append(suffix[-1] + totals[n])
-    suffix = suffix[::-1][1:]
-    to_end = jnp.concatenate([suffix[n] + totals[n] - part(cumul, n) for n in range(blocks)], axis=0)
-    from_start = jnp.concatenate([offsets[n] + part(before, n) for n in range(blocks)], axis=0)
-    fwd_device = mm_tn(value, (key_f * jnp.exp(to_end)).astype(BF16))
-    back_device = mm_tn(value, (key_f * jnp.exp(from_start)).astype(BF16))
-
-    marks = log_rows(whole)
+    fwd_device = mm_tn(value, (key_f * to_end).astype(BF16))
+    back_device = mm_tn(value, (key_f * from_start).astype(BF16))
+
     for q in range(NY):
         SS[q * 144 : q * 144 + 64, :] = fwd_device[q * 64 : q * 64 + 64].astype(BF16)
         SS[q * 144 + 64 : q * 144 + 128, :] = back_device[q * 64 : q * 64 + 64].astype(BF16)
@@ -269,15 +318,12 @@
     for d in range(1, NY):
         send(SS.at[message(d)], R1.at[message()], ("s1", d), at(dy=d))
 
-    qcg = mm(normed, WB[:, 0:640])
-    query_f = (qcg[:, :KEY_DIM] * (1.0 / math.sqrt(KEY_DIM))).astype(BF16).astype(F32)
-    conv_in = qcg[:, KEY_DIM : KEY_DIM + 256].astype(BF16)
-    gate = qcg[:, KEY_DIM + 256 :].astype(BF16).astype(F32)
-    CI[...] = conv_in
-    CP[8 : 8 + LEN, :] = conv_in.astype(F32)
-    send(CI.at[pl.ds(LEN - 16, 16)], HP, "hp", next_dev)
-    send(CI.at[pl.ds(0, 16)], HN, "hn", prev_dev)
-
+    ring_b.step(8)
+    ring_c.fan_out(0)
+    ring_b.columns(8)
+    ring_c.step(1)
+    ring_b.column(8)
+    ring_c.columns(1)
     for d in range(1, NY):
         arrived(R1.at[message(-d)], ("s1", d))
     in_f, in_b, in_l = [], [], []
@@ -311,6 +357,20 @@
     for d in (8, 7, 9, 6, 10, 5, 11, 4, 12, 3, 13, 2, 14, 1, 15):
         start = pl.multiple_of(((z + d) // NZ) * 80, 16)
         send(M2.at[pl.ds(start, 80)], R2.at[depth()], ("s2", d), at(dz=d))
+
+    ring_c.step(2)
+    ring_b.finish()
+    qcg = mm(normed, WB[...])
+    query_f = (qcg[:, :KEY_DIM] * (1.0 / math.sqrt(KEY_DIM))).astype(BF16).astype(F32)
+    conv_in = qcg[:, KEY_DIM : KEY_DIM + 256].astype(BF16)
+    gate = qcg[:, KEY_DIM + 256 :].astype(BF16).astype(F32)
+    CI[...] = conv_in
+    CP[8 : 8 + LEN, :] = conv_in.astype(F32)
+    send(CI.at[pl.ds(LEN - 16, 16)], HP, "hp", next_dev)
+    send(CI.at[pl.ds(0, 16)], HN, "hn", prev_dev)
+    ring_c.columns(2)
+    ring_c.step(3)
+    ring_c.columns(3)
 
     lower = lax.broadcasted_iota(jnp.int32, (BLOCK, BLOCK), 0) >= lax.broadcasted_iota(jnp.int32, (BLOCK, BLOCK), 1)
     upper = lax.broadcasted_iota(jnp.int32, (BLOCK, BLOCK), 0) <= lax.broadcasted_iota(jnp.int32, (BLOCK, BLOCK), 1)
@@ -344,6 +404,8 @@
         [part(query_f, n) * jnp.exp(suffix[n] + (totals[n] - part(before, n))) for n in range(blocks)], axis=0
     ).astype(BF16)
 
+    ring_c.step(4)
+    ring_c.columns(4)
     arrived(HP, "hp")
     arrived(HN, "hn")
     first = HP[...].astype(F32)[15:16]
@@ -354,6 +416,10 @@
     mixed = CP[7 : 7 + LEN, :] * tap[0:1] + CP[8 : 8 + LEN, :] * tap[1:2] + CP[9 : 9 + LEN, :] * tap[2:3]
     XC[:, 0:256] = (mixed * (gate * (1.0 / (1.0 + jnp.exp(-gate))))).astype(BF16)
 
+    ring_c.step(5)
+    ring_c.columns(5)
+    ring_c.step(6)
+    ring_c.columns(6)
     for d in range(1, NZ):
         arrived(R2.at[depth(-d)], ("s2", d))
     sum_f = jnp.zeros((64, KEY_DIM), F32)
@@ -379,12 +445,18 @@
         send(M3.at[answer(d, 1)], IB.at[quarter()], ("s3b", d), at(dy=d))
     IF[quarter(), :] = M3[answer(0, 0), :]
     IB[quarter(), :] = M3[answer(0, 1), :]
+    ring_c.step(7)
+    ring_c.columns(7)
+    ring_c.step(8)
+    ring_c.columns(8)
+    ring_c.column(8)
     for d in range(1, NY):
         arrived(IF.at[quarter(-d)], ("s3f", d))
         arrived(IB.at[quarter(-d)], ("s3b", d))
     raw = local + mm_nt(far_fwd, IF[...]) + mm_nt(far_back, IB[...])
     norm = lax.rsqrt(jnp.mean(raw * raw, axis=-1, keepdims=True) + EPSILON)
     XC[:, 256:512] = (raw * norm * hgain[:, val_cols]).astype(BF16)
+    ring_c.finish()
 
     def block4(r):
         return pl.ds(r * ROWS, ROWS)
@@ -393,11 +465,11 @@
     there = jnp.concatenate([XC[token_rows(dx=r, flip=True), :] for r in order], axis=0)
     here = jnp.concatenate([XC[token_rows(dx=r), :] for r in order], axis=0)
     for n in range(0, WIDTH, 512):
-        PS[:, n : n + 512] = mm_nt(there, WB[n : n + 512, 640:1152]).astype(BF16)
+        PS[:, n : n + 512] = mm_nt(there, WC[n : n + 512, :]).astype(BF16)
     for i in range(4):
         send(PS.at[block4(i)], PR.at[block4(i)], ("pr", i), at(flip=True))
     for n in range(0, WIDTH, 512):
-        PO[:, n : n + 512] = mm_nt(here, WB[n : n + 512, 640:1152])
+        PO[:, n : n + 512] = mm_nt(here, WC[n : n + 512, :])
     for i in range(3):
         arrived(PR.at[block4(i)], ("pr", i))
         XS[i * ROWS : (i + 1) * ROWS, :] = (
@@ -420,19 +492,24 @@
     tokens, norm_gain, conv_in_weight, conv_gate_weight, conv_taps, query_weight, key_weight, value_weight,
     decay_down, decay_up, decay_bias, decay_extra, head_gain, conv_out_weight, value_out_weight,
 ):
-    wa = jnp.concatenate([key_weight, value_weight], axis=1)
-    wb = jnp.concatenate(
-        [query_weight, conv_in_weight, conv_gate_weight, conv_out_weight.T, value_out_weight.T], axis=1
-    )
-    vmem = pl.BlockSpec(memory_space=pltpu.VMEM)
+    hbm = pl.BlockSpec(memory_space=pl.ANY)
     return pl.pallas_call(
         kernel,
         out_shape=jax.ShapeDtypeStruct((ROWS, WIDTH), BF16),
-        in_specs=[vmem] * 10,
-        out_specs=vmem,
+        in_specs=[hbm] * 15,
+        out_specs=pl.BlockSpec(memory_space=pltpu.VMEM),
         scratch_shapes=[
+            pltpu.VMEM((ROWS, WIDTH), BF16),
+            pltpu.VMEM((1, WIDTH), F32),
+            pltpu.VMEM((3, WIDTH), F32),
+            pltpu.VMEM((16, WIDTH), BF16),
+            pltpu.VMEM((16, 1024), BF16),
+            pltpu.VMEM((1, 1024), F32),
+            pltpu.VMEM((1, LEN), F32),
+            pltpu.VMEM((1, WIDTH), F32),
             pltpu.VMEM((2048, 384), BF16),
-            pltpu.VMEM((2048, 1152), BF16),
+            pltpu.VMEM((2048, 640), BF16),
+            pltpu.VMEM((2048, 512), BF16),
             pltpu.VMEM((LEN, WIDTH), BF16),
             pltpu.VMEM((NY * 144, KEY_DIM), BF16),
             pltpu.VMEM((NY * 144, KEY_DIM), BF16),
@@ -453,12 +530,14 @@
             pltpu.VMEM((3 * ROWS, WIDTH), BF16),
             pltpu.SemaphoreType.DMA((N_SEND,)),
             pltpu.SemaphoreType.DMA((N_RECV,)),
+            pltpu.SemaphoreType.DMA((15,)),
         ],
         compiler_params=pltpu.CompilerParams(collective_id=0, has_side_effects=True, vmem_limit_bytes=60 * 1024 * 1024),
         cost_estimate=pl.CostEstimate(flops=3_000_000_000, bytes_accessed=1_000_000, transcendentals=0),
     )(
-        tokens, norm_gain.reshape(1, -1), wa, wb, conv_taps, decay_down, decay_up,
-        decay_bias.reshape(1, -1), decay_extra, head_gain.reshape(1, -1),
+        tokens, norm_gain.reshape(1, -1), conv_in_weight, conv_gate_weight, conv_taps, query_weight, key_weight,
+        value_weight, decay_down.T, decay_up, decay_bias.reshape(1, -1), decay_extra, head_gain.reshape(1, -1),
+        conv_out_weight.T, value_out_weight.T,
     )
 
 

time: 116 us -> 111 us (0.957)
  local copies, waits for them, and re-layouts: 4.16 us -> 1.62 us
  other arithmetic: 1.35 us -> 0 us
    unnamed x20 -> x1, local copies, waits for them, and re-layouts: 4.16 us -> 1.62 us
    concatenate x1 -> x0, other arithmetic: 1.35 us -> none  [local(): wa = jnp.concatenate([key_weight, value_weight], axis=1)]
where the time goes in v2:
time: 111 us
  Pallas kernels  109 us (98%)
  local copies, waits for them, and re-layouts  1.62 us (1%)
    pallas_call x1, Pallas kernels, local(): pl.pallas_call(kernel, out_shape=jax.ShapeDtypeStruct((ROWS, WIDTH), BF16...  109 us

profile of v2, /device:TPU:1, one launch (start us, length us, event | category | flops | bytes accessed | tf_op | source)
XLA Modules:
  0.0 111.0 jit_solution(3373241536013839396)
XLA Ops:
  0.0 109.4 %shard_map.145 = bf16[48,2048]{1,0:T(8,128)(2,1)} custom-call(bf16[48,2048]{1,0:T(8,128)(2,1)} %tok_h.1, f32[1,2048]{1,0:T(1,128)} %bitcast.9, bf16[32,256]{1,0:T(8,128)(2,1)} %ci_h.1, bf16[32,256]{1,0:T(8,128)(2,1)} %cg_h.1, f32[3,2048]{1,0:T(4,128)} %taps_h.1, bf16[32,128]{1,0:T(8,128)(2,1)} %q_h.1, bf16[32,128]{1,0:T(8,128)(2,1)} %k_h.1, ...), custom_call_target="tpu_custom_call" | custom-call | flops 3000000000 | bytes 1000000 | tf_op jit(solution)/shard_map/pallas_call | solution.py:496
  109.4 1.6 %copy.17 = bf16[48,2048]{1,0:T(8,128)(2,1)} copy(bf16[48,2048]{1,0:T(8,128)(2,1)} %shard_map.145) | data formatting | bytes 393216

commit v3 on v2

--- a/solution.py
+++ b/solution.py
@@ -155,70 +155,71 @@
     def place(j):
         return 0 if j == 0 else (-j if j <= 8 else j - 8)
 
-    def plus(j):
-        return (j % 2 == 0) if j <= 8 else ((j - 8) % 2 == 1)
-
     class Ring:
         def __init__(self, W, tag):
             self.W, self.tag = W, tag
 
-        def around(self):
-            ref = self.W.at[slot()]
-            send(ref, ref, (self.tag, "zm", 1), at(dz=1))
-            send(ref, ref, (self.tag, "zp", 1), at(dz=-1))
+        def hop(self, chain, sign, k):
+            ref = self.W.at[slot(-sign * (k - 1), 2 * chain)]
+            send(ref, ref, (self.tag, chain, sign, k), at(dz=sign))
 
         def fan_out(self, j):
             ref = self.W.at[slot(place(j))]
             send(ref, ref, (self.tag, "ym", j), at(dy=1))
             send(ref, ref, (self.tag, "yp", j), at(dy=-1))
 
-        def step(self, k):
-            ref = self.W.at[slot(-k)]
-            arrived(ref, (self.tag, "zm", k))
-            if k < 8:
-                send(ref, ref, (self.tag, "zm", k + 1), at(dz=1))
-            self.fan_out(k)
-            if k < 8:
-                ref = self.W.at[slot(k)]
-                arrived(ref, (self.tag, "zp", k))
-                if k < 7:
-                    send(ref, ref, (self.tag, "zp", k + 1), at(dz=-1))
-                self.fan_out(8 + k)
-
-        def column(self, j):
-            dz = place(j)
-            ref = self.W.at[slot(dz, -1)]
-            arrived(ref, (self.tag, "ym", j))
-            if plus(j):
-                send(ref, ref, (self.tag, "y2", j), at(dy=1))
-            ref = self.W.at[slot(dz, 1)]
-            arrived(ref, (self.tag, "yp", j))
-            if not plus(j):
-                send(ref, ref, (self.tag, "y2", j), at(dy=-1))
-
-        def columns(self, k):
-            self.column(k - 1)
-            if k > 1:
-                self.column(7 + k)
+        def across(self):
+            ref = self.W.at[slot()]
+            send(ref, ref, (self.tag, "y2"), at(dy=2))
+
+        def around(self, chain):
+            if chain:
+                arrived(self.W.at[slot(0, 2)], (self.tag, "y2"))
+            self.hop(chain, 1, 1)
+            self.hop(chain, -1, 1)
+
+        def step(self, k, chains=(0, 1), fan=True):
+            for chain in chains:
+                for sign in (1, -1):
+                    if sign == -1 and k == 8:
+                        continue
+                    arrived(self.W.at[slot(-sign * k, 2 * chain)], (self.tag, chain, sign, k))
+                    if k < (8 if sign == 1 else 7):
+                        self.hop(chain, sign, k + 1)
+                    if chain == 0 and fan:
+                        self.fan_out(k if sign == 1 else 8 + k)
+
+        def column(self, *js):
+            for j in js:
+                plus = (j % 2 == 0) if j <= 8 else ((j - 8) % 2 == 1)
+                for dy, name in ((-1, "ym"), (1, "yp")):
+                    ref = self.W.at[slot(place(j), dy)]
+                    arrived(ref, (self.tag, name, j))
+                    if plus == (dy == -1):
+                        send(ref, ref, (self.tag, "y2", j), at(dy=-dy))
+
+        def last_column(self):
+            for j in range(16):
+                arrived(self.W.at[slot(place(j), 2)], (self.tag, "y2", j))
 
         def finish(self):
             for j in range(16):
-                arrived(self.W.at[slot(place(j), 2)], (self.tag, "y2", j))
-
-    ring_b, ring_c = Ring(WB, "b"), Ring(WC, "c")
-    own_a = WA.at[slot()]
-    for d in range(1, NY):
-        send(own_a, own_a, ("ay", d), at(dy=d))
+                arrived(self.W.at[slot(place(j), -1)], (self.tag, "ym", j))
+                arrived(self.W.at[slot(place(j), 1)], (self.tag, "yp", j))
+
+    ring_a, ring_b, ring_c = Ring(WA, "a"), Ring(WB, "b"), Ring(WC, "c")
+    ring_a.across()
+    ring_a.around(0)
+    ring_a.fan_out(0)
     own_rows = T.at[token_rows()]
     send(own_rows, own_rows, "tm", at(dx=1))
     send(own_rows, own_rows, "tp", at(dx=-1))
     send(own_rows, own_rows, ("tc", 0), at(flip=True))
-    ring_b.around()
+    ring_b.across()
+    ring_b.around(0)
     ring_b.fan_out(0)
-    for d in range(1, NY):
-        arrived(WA.at[slot(dy=-d)], ("ay", d))
-    send(WA.at[plane()], WA.at[plane()], ("am", 1), at(dz=1))
-    send(WA.at[plane()], WA.at[plane()], ("ap", 1), at(dz=-1))
+    ring_c.around(0)
+    ring_c.fan_out(0)
 
     half = WIDTH // 2
     blocks = LEN // BLOCK
@@ -264,22 +265,25 @@
         return cumul, cumul - log_decay
 
     for k in range(1, 9):
-        ref = WA.at[plane(-k)]
-        arrived(ref, ("am", k))
-        if k < 8:
-            send(ref, ref, ("am", k + 1), at(dz=1))
-            ref = WA.at[plane(k)]
-            arrived(ref, ("ap", k))
-            if k < 7:
-                send(ref, ref, ("ap", k + 1), at(dz=-1))
-        if k < 8:
-            ring_b.step(k)
-        if k == 2:
+        ring_a.step(k, (0,))
+        if k == 1:
+            ring_a.around(1)
+        else:
+            ring_a.step(k - 1, (1,))
+        ring_b.step(k, (0,))
+        if k == 1:
+            ring_b.around(1)
+        else:
+            ring_b.step(k - 1, (1,))
+        ring_c.step(k, (0,), fan=k <= 4)
+        if k == 1:
             token_step(0)
+        if k == 3:
+            token_step(1)
         if k == 4:
-            token_step(1)
-        if k < 8:
-            ring_b.columns(k)
+            ring_c.column(0)
+        if k > 4:
+            ring_c.column(k - 4, k + 4)
         if k == 6:
             token_step(2)
             cumul, before = decay()
@@ -296,8 +300,8 @@
             from_start = jnp.concatenate([offsets[n] + part(before, n) for n in range(blocks)], axis=0)
             to_end, from_start = jnp.exp(to_end), jnp.exp(from_start)
             marks = log_rows(whole)
-        if k == 7:
-            ring_c.around()
+    ring_a.step(8, (1,))
+    ring_a.finish()
 
     normed = T[...]
     kv = mm(normed, WA[...])
@@ -318,12 +322,9 @@
     for d in range(1, NY):
         send(SS.at[message(d)], R1.at[message()], ("s1", d), at(dy=d))
 
-    ring_b.step(8)
-    ring_c.fan_out(0)
-    ring_b.columns(8)
-    ring_c.step(1)
-    ring_b.column(8)
-    ring_c.columns(1)
+    ring_b.step(8, (1,))
+    ring_c.fan_out(5)
+    ring_c.fan_out(13)
     for d in range(1, NY):
         arrived(R1.at[message(-d)], ("s1", d))
     in_f, in_b, in_l = [], [], []
@@ -358,7 +359,8 @@
         start = pl.multiple_of(((z + d) // NZ) * 80, 16)
         send(M2.at[pl.ds(start, 80)], R2.at[depth()], ("s2", d), at(dz=d))
 
-    ring_c.step(2)
+    ring_c.fan_out(6)
+    ring_c.fan_out(14)
     ring_b.finish()
     qcg = mm(normed, WB[...])
     query_f = (qcg[:, :KEY_DIM] * (1.0 / math.sqrt(KEY_DIM))).astype(BF16).astype(F32)
@@ -368,9 +370,10 @@
     CP[8 : 8 + LEN, :] = conv_in.astype(F32)
     send(CI.at[pl.ds(LEN - 16, 16)], HP, "hp", next_dev)
     send(CI.at[pl.ds(0, 16)], HN, "hn", prev_dev)
-    ring_c.columns(2)
-    ring_c.step(3)
-    ring_c.columns(3)
+    ring_c.column(5, 13)
+    ring_c.fan_out(7)
+    ring_c.fan_out(15)
+    ring_c.fan_out(8)
 
     lower = lax.broadcasted_iota(jnp.int32, (BLOCK, BLOCK), 0) >= lax.broadcasted_iota(jnp.int32, (BLOCK, BLOCK), 1)
     upper = lax.broadcasted_iota(jnp.int32, (BLOCK, BLOCK), 0) <= lax.broadcasted_iota(jnp.int32, (BLOCK, BLOCK), 1)
@@ -404,8 +407,7 @@
         [part(query_f, n) * jnp.exp(suffix[n] + (totals[n] - part(before, n))) for n in range(blocks)], axis=0
     ).astype(BF16)
 
-    ring_c.step(4)
-    ring_c.columns(4)
+    ring_c.column(6, 14)
     arrived(HP, "hp")
     arrived(HN, "hn")
     first = HP[...].astype(F32)[15:16]
@@ -416,10 +418,7 @@
     mixed = CP[7 : 7 + LEN, :] * tap[0:1] + CP[8 : 8 + LEN, :] * tap[1:2] + CP[9 : 9 + LEN, :] * tap[2:3]
     XC[:, 0:256] = (mixed * (gate * (1.0 / (1.0 + jnp.exp(-gate))))).astype(BF16)
 
-    ring_c.step(5)
-    ring_c.columns(5)
-    ring_c.step(6)
-    ring_c.columns(6)
+    ring_c.column(7, 15, 8)
     for d in range(1, NZ):
         arrived(R2.at[depth(-d)], ("s2", d))
     sum_f = jnp.zeros((64, KEY_DIM), F32)
@@ -445,43 +444,47 @@
         send(M3.at[answer(d, 1)], IB.at[quarter()], ("s3b", d), at(dy=d))
     IF[quarter(), :] = M3[answer(0, 0), :]
     IB[quarter(), :] = M3[answer(0, 1), :]
-    ring_c.step(7)
-    ring_c.columns(7)
-    ring_c.step(8)
-    ring_c.columns(8)
-    ring_c.column(8)
     for d in range(1, NY):
         arrived(IF.at[quarter(-d)], ("s3f", d))
         arrived(IB.at[quarter(-d)], ("s3b", d))
     raw = local + mm_nt(far_fwd, IF[...]) + mm_nt(far_back, IB[...])
     norm = lax.rsqrt(jnp.mean(raw * raw, axis=-1, keepdims=True) + EPSILON)
     XC[:, 256:512] = (raw * norm * hgain[:, val_cols]).astype(BF16)
-    ring_c.finish()
-
-    def block4(r):
-        return pl.ds(r * ROWS, ROWS)
+    ring_c.last_column()
 
     order = (2, 1, 3, 0)
+    pieces, piece = 4, WIDTH // 4
     there = jnp.concatenate([XC[token_rows(dx=r, flip=True), :] for r in order], axis=0)
     here = jnp.concatenate([XC[token_rows(dx=r), :] for r in order], axis=0)
-    for n in range(0, WIDTH, 512):
-        PS[:, n : n + 512] = mm_nt(there, WC[n : n + 512, :]).astype(BF16)
-    for i in range(4):
-        send(PS.at[block4(i)], PR.at[block4(i)], ("pr", i), at(flip=True))
-    for n in range(0, WIDTH, 512):
-        PO[:, n : n + 512] = mm_nt(here, WC[n : n + 512, :])
-    for i in range(3):
-        arrived(PR.at[block4(i)], ("pr", i))
-        XS[i * ROWS : (i + 1) * ROWS, :] = (
-            PO[i * ROWS : (i + 1) * ROWS, :] + PR[i * ROWS : (i + 1) * ROWS, :].astype(F32)
-        ).astype(BF16)
-        send(XS.at[block4(i)], XR.at[block4(i)], ("xr", i), at(dx=order[i]))
-    arrived(PR.at[block4(3)], ("pr", 3))
-    total = PO[3 * ROWS :, :] + PR[3 * ROWS :, :].astype(F32)
-    for i in (1, 2, 0):
-        arrived(XR.at[block4(i)], ("xr", i))
-        total = total + XR[i * ROWS : (i + 1) * ROWS, :].astype(F32)
-    out[...] = total.astype(BF16)
+
+    def rows4(n, i=0, count=4):
+        return pl.ds((n * 4 + i) * ROWS, count * ROWS)
+
+    def pair_send(n):
+        PS[rows4(n), :] = mm_nt(there, WC[n * piece : (n + 1) * piece, :]).astype(BF16)
+        send(PS.at[rows4(n)], PR.at[rows4(n)], ("pr", n), at(flip=True))
+
+    def x_send(n):
+        mine = mm_nt(here, WC[n * piece : (n + 1) * piece, :])
+        arrived(PR.at[rows4(n)], ("pr", n))
+        both = mine + PR[rows4(n), :].astype(F32)
+        XS[rows4(n), :] = both.astype(BF16)
+        for i in range(3):
+            send(XS.at[rows4(n, i, 1)], XR.at[rows4(n, i, 1)], ("xr", n, i), at(dx=order[i]))
+        PO[pl.ds(n * ROWS, ROWS), :] = both[3 * ROWS :]
+
+    pair_send(0)
+    pair_send(1)
+    for n in range(pieces):
+        x_send(n)
+        if n + 2 < pieces:
+            pair_send(n + 2)
+    for n in range(pieces):
+        total = PO[n * ROWS : (n + 1) * ROWS, :]
+        for i in (1, 2, 0):
+            arrived(XR.at[rows4(n, i, 1)], ("xr", n, i))
+            total = total + XR[rows4(n, i, 1), :].astype(F32)
+        out[:, n * piece : (n + 1) * piece] = total.astype(BF16)
 
     for copy in sends:
         copy.wait_send()
@@ -523,11 +526,11 @@
             pltpu.VMEM((16, 256), BF16),
             pltpu.VMEM((16, 256), BF16),
             pltpu.VMEM((LEN, 512), BF16),
-            pltpu.VMEM((4 * ROWS, WIDTH), F32),
-            pltpu.VMEM((4 * ROWS, WIDTH), BF16),
-            pltpu.VMEM((4 * ROWS, WIDTH), BF16),
-            pltpu.VMEM((3 * ROWS, WIDTH), BF16),
-            pltpu.VMEM((3 * ROWS, WIDTH), BF16),
+            pltpu.VMEM((4 * ROWS, WIDTH // 4), F32),
+            pltpu.VMEM((16 * ROWS, WIDTH // 4), BF16),
+            pltpu.VMEM((16 * ROWS, WIDTH // 4), BF16),
+            pltpu.VMEM((16 * ROWS, WIDTH // 4), BF16),
+            pltpu.VMEM((16 * ROWS, WIDTH // 4), BF16),
             pltpu.SemaphoreType.DMA((N_SEND,)),
             pltpu.SemaphoreType.DMA((N_RECV,)),
             pltpu.SemaphoreType.DMA((15,)),

time: 111 us -> 93.3 us (0.84)
  Pallas kernels: 109 us -> 91.5 us
    pallas_call x1, Pallas kernels: 109 us -> 91.5 us  [local(): pl.pallas_call(kernel, out_shape=jax.ShapeDtypeStruct((ROWS, WIDTH), BF16...]
where the time goes in v3:
time: 93.3 us; the launch traced here: 93.1 us
  Pallas kernels  91.5 us (98%)
  local copies, waits for them, and re-layouts  1.62 us (2%)
    pallas_call x1, Pallas kernels, local(): pl.pallas_call(kernel, out_shape=jax.ShapeDtypeStruct((ROWS, WIDTH), BF16...  91.5 us

profile of v3, /device:TPU:1, one launch (start us, length us, event | category | flops | bytes accessed | tf_op | source)
XLA Modules:
  0.0 93.1 jit_solution(14816483217109858520)
XLA Ops:
  0.0 91.5 %shard_map.145 = bf16[48,2048]{1,0:T(8,128)(2,1)} custom-call(bf16[48,2048]{1,0:T(8,128)(2,1)} %tok_h.1, f32[1,2048]{1,0:T(1,128)} %bitcast.9, bf16[32,256]{1,0:T(8,128)(2,1)} %ci_h.1, bf16[32,256]{1,0:T(8,128)(2,1)} %cg_h.1, f32[3,2048]{1,0:T(4,128)} %taps_h.1, bf16[32,128]{1,0:T(8,128)(2,1)} %q_h.1, bf16[32,128]{1,0:T(8,128)(2,1)} %k_h.1, ...), custom_call_target="tpu_custom_call" | custom-call | flops 3000000000 | bytes 1000000 | tf_op jit(solution)/shard_map/pallas_call | solution.py:499
  91.5 1.6 %copy.17 = bf16[48,2048]{1,0:T(8,128)(2,1)} copy(bf16[48,2048]{1,0:T(8,128)(2,1)} %shard_map.145) | data formatting | bytes 393216

commit v4 on v3

--- a/solution.py
+++ b/solution.py
@@ -67,7 +67,7 @@
     tok_h, gain_h, ci_h, cg_h, taps_h, q_h, k_h, v_h, dd_h, du_h, db_h, de_h, hg_h, co_h, vo_h,
     out,
     tok, norm_gain, taps, ddown, dup, dbias, dextra, hgain,
-    WA, WB, WC, T, SS, R1, M2, R2, M3, IF, IB, CI, CP, HP, HN, XC, PO, PS, PR, XS, XR,
+    WA, WB, WC, T, SS, R1, M2, NEAR, M4, R2, M3, IF, IB, CI, CP, HP, HN, XC, PO, PS, PR, XS, XR,
     ssem, rsem, lsem,
 ):
     z, y, x, c = (lax.axis_index(a) for a in SP_TP)
@@ -101,7 +101,7 @@
     ahead = lax.rem(s + NZ * NY - 1, NZ * NY)
     next_dev = (after // NY, lax.rem(after, NY), x, c)
     prev_dev = (ahead // NY, lax.rem(ahead, NY), x, c)
-    peers = [at(dz=d) for d in (1, -1)]
+    peers = [at(dz=d) for d in (1, -1, 2, -2)]
     peers += [at(dy=d) for d in range(1, NY)]
     peers += [at(dx=d) for d in range(1, NX)]
     peers += [at(flip=True), next_dev, prev_dev]
@@ -207,9 +207,27 @@
                 arrived(self.W.at[slot(place(j), -1)], (self.tag, "ym", j))
                 arrived(self.W.at[slot(place(j), 1)], (self.tag, "yp", j))
 
-    ring_a, ring_b, ring_c = Ring(WA, "a"), Ring(WB, "b"), Ring(WC, "c")
-    ring_a.across()
-    ring_a.around(0)
+    class Jumps(Ring):
+        def leap(self, sign, base):
+            ref = self.W.at[slot(-sign * base)]
+            for d in (2, 1):
+                if base + d <= (8 if sign == 1 else 7):
+                    send(ref, ref, (self.tag, 0, sign, base + d), at(dz=sign * d))
+
+        def stage(self, i):
+            for d in (2, 1):
+                for sign in (1, -1):
+                    k = 2 * i - 2 + d
+                    if k > (8 if sign == 1 else 7):
+                        continue
+                    arrived(self.W.at[slot(-sign * k)], (self.tag, 0, sign, k))
+                    if d == 2:
+                        self.leap(sign, k)
+                    self.fan_out(k if sign == 1 else 8 + k)
+
+    ring_a, ring_b, ring_c = Jumps(WA, "a"), Ring(WB, "b"), Ring(WC, "c")
+    ring_a.leap(1, 0)
+    ring_a.leap(-1, 0)
     ring_a.fan_out(0)
     own_rows = T.at[token_rows()]
     send(own_rows, own_rows, "tm", at(dx=1))
@@ -217,9 +235,24 @@
     send(own_rows, own_rows, ("tc", 0), at(flip=True))
     ring_b.across()
     ring_b.around(0)
+    ring_c.across()
+    ring_c.around(0)
     ring_b.fan_out(0)
-    ring_c.around(0)
-    ring_c.fan_out(0)
+
+    def weights_step(k, fan=True):
+        if k <= 8:
+            ring_b.step(k, (0,))
+            ring_c.step(k, (0,), fan=fan)
+        if k == 1:
+            ring_b.around(1)
+            ring_c.around(1)
+        else:
+            ring_b.step(k - 1, (1,))
+            ring_c.step(k - 1, (1,))
+
+    def late_fan(*js):
+        for j in js:
+            ring_c.fan_out(j)
 
     half = WIDTH // 2
     blocks = LEN // BLOCK
@@ -264,44 +297,41 @@
         )
         return cumul, cumul - log_decay
 
-    for k in range(1, 9):
-        ring_a.step(k, (0,))
-        if k == 1:
-            ring_a.around(1)
-        else:
-            ring_a.step(k - 1, (1,))
-        ring_b.step(k, (0,))
-        if k == 1:
-            ring_b.around(1)
-        else:
-            ring_b.step(k - 1, (1,))
-        ring_c.step(k, (0,), fan=k <= 4)
-        if k == 1:
-            token_step(0)
-        if k == 3:
-            token_step(1)
-        if k == 4:
-            ring_c.column(0)
-        if k > 4:
-            ring_c.column(k - 4, k + 4)
-        if k == 6:
-            token_step(2)
-            cumul, before = decay()
-            totals = [cumul[(n + 1) * BLOCK - 1 : (n + 1) * BLOCK] for n in range(blocks)]
-            offsets = [jnp.zeros((1, KEY_DIM), F32)]
-            for n in range(blocks):
-                offsets.append(offsets[-1] + totals[n])
-            whole = offsets[blocks]
-            suffix = [jnp.zeros((1, KEY_DIM), F32)]
-            for n in reversed(range(blocks)):
-                suffix.append(suffix[-1] + totals[n])
-            suffix = suffix[::-1][1:]
-            to_end = jnp.concatenate([suffix[n] + totals[n] - part(cumul, n) for n in range(blocks)], axis=0)
-            from_start = jnp.concatenate([offsets[n] + part(before, n) for n in range(blocks)], axis=0)
-            to_end, from_start = jnp.exp(to_end), jnp.exp(from_start)
-            marks = log_rows(whole)
-    ring_a.step(8, (1,))
-    ring_a.finish()
+    ring_a.stage(1)
+    ring_a.column(0)
+    weights_step(1, fan=False)
+    token_step(0)
+    ring_a.stage(2)
+    ring_a.column(1, 9)
+    weights_step(2, fan=False)
+    ring_a.column(2, 10)
+    ring_a.stage(3)
+    ring_a.column(3, 11)
+    token_step(1)
+    weights_step(3, fan=False)
+    ring_a.column(4, 12)
+    ring_a.stage(4)
+    ring_a.column(5, 13)
+    token_step(2)
+    cumul, before = decay()
+    totals = [cumul[(n + 1) * BLOCK - 1 : (n + 1) * BLOCK] for n in range(blocks)]
+    offsets = [jnp.zeros((1, KEY_DIM), F32)]
+    for n in range(blocks):
+        offsets.append(offsets[-1] + totals[n])
+    whole = offsets[blocks]
+    suffix = [jnp.zeros((1, KEY_DIM), F32)]
+    for n in reversed(range(blocks)):
+        suffix.append(suffix[-1] + totals[n])
+    suffix = suffix[::-1][1:]
+    to_end = jnp.concatenate([suffix[n] + totals[n] - part(cumul, n) for n in range(blocks)], axis=0)
+    from_start = jnp.concatenate([offsets[n] + part(before, n) for n in range(blocks)], axis=0)
+    to_end, from_start = jnp.exp(to_end), jnp.exp(from_start)
+    marks = log_rows(whole)
+    weights_step(4, fan=False)
+    ring_a.column(6, 14)
+    ring_a.column(7, 15, 8)
+    weights_step(5, fan=False)
+    ring_a.last_column()
 
     normed = T[...]
     kv = mm(normed, WA[...])
@@ -322,9 +352,8 @@
     for d in range(1, NY):
         send(SS.at[message(d)], R1.at[message()], ("s1", d), at(dy=d))
 
-    ring_b.step(8, (1,))
-    ring_c.fan_out(5)
-    ring_c.fan_out(13)
+    late_fan(0, 1, 9)
+    weights_step(6)
     for d in range(1, NY):
         arrived(R1.at[message(-d)], ("s1", d))
     in_f, in_b, in_l = [], [], []
@@ -355,12 +384,29 @@
         return pl.ds(pl.multiple_of(wrap(z + dz, NZ) * 80, 16), 80)
 
     R2[depth(), :] = M2[0:80, :]
-    for d in (8, 7, 9, 6, 10, 5, 11, 4, 12, 3, 13, 2, 14, 1, 15):
+    send(M2.at[pl.ds(0, 80)], NEAR.at[pl.ds(0, 80)], "s2f", at(dz=1))
+    send(M2.at[pl.ds(80, 80)], NEAR.at[pl.ds(80, 80)], "s2b", at(dz=-1))
+    late_fan(2, 10)
+    weights_step(7)
+    arrived(NEAR.at[pl.ds(0, 80)], "s2f")
+    arrived(NEAR.at[pl.ds(80, 80)], "s2b")
+    near_f = jnp.where(z > 0, NEAR[0:64, :].astype(F32), 0.0)
+    near_b = jnp.where(z < NZ - 1, NEAR[80:144, :].astype(F32), 0.0)
+    near_lf, near_lb = log_total(NEAR[64:80, :]), log_total(NEAR[144:160, :])
+    fade = jnp.exp(log_f)
+    M4[0:64, :] = (total_f + fade * near_f).astype(BF16)
+    M4[64:80, :] = log_rows(log_f + near_lf)
+    M4[80:144, :] = (total_b + fade * near_b).astype(BF16)
+    M4[144:160, :] = log_rows(log_f + near_lb)
+    for d in (8, 6, 10, 4, 12, 2, 14):
         start = pl.multiple_of(((z + d) // NZ) * 80, 16)
-        send(M2.at[pl.ds(start, 80)], R2.at[depth()], ("s2", d), at(dz=d))
-
-    ring_c.fan_out(6)
-    ring_c.fan_out(14)
+        send(M4.at[pl.ds(start, 80)], R2.at[depth()], ("s2", d), at(dz=d))
+
+    late_fan(3, 11)
+    weights_step(8)
+    late_fan(4, 12)
+    weights_step(9)
+    late_fan(5, 13)
     ring_b.finish()
     qcg = mm(normed, WB[...])
     query_f = (qcg[:, :KEY_DIM] * (1.0 / math.sqrt(KEY_DIM))).astype(BF16).astype(F32)
@@ -370,11 +416,34 @@
     CP[8 : 8 + LEN, :] = conv_in.astype(F32)
     send(CI.at[pl.ds(LEN - 16, 16)], HP, "hp", next_dev)
     send(CI.at[pl.ds(0, 16)], HN, "hn", prev_dev)
-    ring_c.column(5, 13)
-    ring_c.fan_out(7)
-    ring_c.fan_out(15)
-    ring_c.fan_out(8)
-
+    for d in range(2, NZ, 2):
+        arrived(R2.at[depth(-d)], ("s2", d))
+    sum_f = jnp.zeros((64, KEY_DIM), F32)
+    sum_b = jnp.zeros((64, KEY_DIM), F32)
+    for d in range(NZ - 2, 0, -2):
+        got = R2[depth(-d), :]
+        step = jnp.exp(log_total(got[64:80])) * sum_f + got[0:64].astype(F32)
+        sum_f = jnp.where(z >= d, step, sum_f)
+        got = R2[depth(d), :]
+        step = jnp.exp(log_total(got[64:80])) * sum_b + got[0:64].astype(F32)
+        sum_b = jnp.where(z + d < NZ, step, sum_b)
+    sum_f = jnp.where(z > 0, jnp.exp(near_lf) * sum_f + near_f, 0.0)
+    sum_b = jnp.where(z < NZ - 1, jnp.exp(near_lb) * sum_b + near_b, 0.0)
+    for q in range(NY):
+        M3[q * 128 : q * 128 + 64, :] = (plane_f[q] + jnp.exp(gap_f[q]) * sum_f).astype(BF16)
+        M3[q * 128 + 64 : q * 128 + 128, :] = (plane_b[q] + jnp.exp(gap_b[q]) * sum_b).astype(BF16)
+
+    def quarter(dy=0):
+        return pl.ds(pl.multiple_of(wrap(y + dy, NY) * 64, 64), 64)
+
+    def answer(dy, which):
+        return pl.ds(pl.multiple_of(wrap(y + dy, NY) * 128 + 64 * which, 64), 64)
+
+    for d in range(1, NY):
+        send(M3.at[answer(d, 0)], IF.at[quarter()], ("s3f", d), at(dy=d))
+        send(M3.at[answer(d, 1)], IB.at[quarter()], ("s3b", d), at(dy=d))
+    IF[quarter(), :] = M3[answer(0, 0), :]
+    IB[quarter(), :] = M3[answer(0, 1), :]
     lower = lax.broadcasted_iota(jnp.int32, (BLOCK, BLOCK), 0) >= lax.broadcasted_iota(jnp.int32, (BLOCK, BLOCK), 1)
     upper = lax.broadcasted_iota(jnp.int32, (BLOCK, BLOCK), 0) <= lax.broadcasted_iota(jnp.int32, (BLOCK, BLOCK), 1)
     within = []
@@ -407,7 +476,6 @@
         [part(query_f, n) * jnp.exp(suffix[n] + (totals[n] - part(before, n))) for n in range(blocks)], axis=0
     ).astype(BF16)
 
-    ring_c.column(6, 14)
     arrived(HP, "hp")
     arrived(HN, "hn")
     first = HP[...].astype(F32)[15:16]
@@ -418,39 +486,13 @@
     mixed = CP[7 : 7 + LEN, :] * tap[0:1] + CP[8 : 8 + LEN, :] * tap[1:2] + CP[9 : 9 + LEN, :] * tap[2:3]
     XC[:, 0:256] = (mixed * (gate * (1.0 / (1.0 + jnp.exp(-gate))))).astype(BF16)
 
-    ring_c.column(7, 15, 8)
-    for d in range(1, NZ):
-        arrived(R2.at[depth(-d)], ("s2", d))
-    sum_f = jnp.zeros((64, KEY_DIM), F32)
-    sum_b = jnp.zeros((64, KEY_DIM), F32)
-    for k in range(NZ):
-        step = jnp.exp(log_total(R2[k * 80 + 64 : k * 80 + 80, :])) * sum_f + R2[k * 80 : k * 80 + 64, :].astype(F32)
-        sum_f = jnp.where(k < z, step, sum_f)
-    for k in reversed(range(NZ)):
-        step = jnp.exp(log_total(R2[k * 80 + 64 : k * 80 + 80, :])) * sum_b + R2[k * 80 : k * 80 + 64, :].astype(F32)
-        sum_b = jnp.where(k > z, step, sum_b)
-    for q in range(NY):
-        M3[q * 128 : q * 128 + 64, :] = (plane_f[q] + jnp.exp(gap_f[q]) * sum_f).astype(BF16)
-        M3[q * 128 + 64 : q * 128 + 128, :] = (plane_b[q] + jnp.exp(gap_b[q]) * sum_b).astype(BF16)
-
-    def quarter(dy=0):
-        return pl.ds(pl.multiple_of(wrap(y + dy, NY) * 64, 64), 64)
-
-    def answer(dy, which):
-        return pl.ds(pl.multiple_of(wrap(y + dy, NY) * 128 + 64 * which, 64), 64)
-
-    for d in range(1, NY):
-        send(M3.at[answer(d, 0)], IF.at[quarter()], ("s3f", d), at(dy=d))
-        send(M3.at[answer(d, 1)], IB.at[quarter()], ("s3b", d), at(dy=d))
-    IF[quarter(), :] = M3[answer(0, 0), :]
-    IB[quarter(), :] = M3[answer(0, 1), :]
     for d in range(1, NY):
         arrived(IF.at[quarter(-d)], ("s3f", d))
         arrived(IB.at[quarter(-d)], ("s3b", d))
     raw = local + mm_nt(far_fwd, IF[...]) + mm_nt(far_back, IB[...])
     norm = lax.rsqrt(jnp.mean(raw * raw, axis=-1, keepdims=True) + EPSILON)
     XC[:, 256:512] = (raw * norm * hgain[:, val_cols]).astype(BF16)
-    ring_c.last_column()
+    ring_c.finish()
 
     order = (2, 1, 3, 0)
     pieces, piece = 4, WIDTH // 4
@@ -517,6 +559,8 @@
             pltpu.VMEM((NY * 144, KEY_DIM), BF16),
             pltpu.VMEM((NY * 144, KEY_DIM), BF16),
             pltpu.VMEM((160, KEY_DIM), BF16),
+            pltpu.VMEM((160, KEY_DIM), BF16),
+            pltpu.VMEM((160, KEY_DIM), BF16),
             pltpu.VMEM((NZ * 80, KEY_DIM), BF16),
             pltpu.VMEM((NY * 128, KEY_DIM), BF16),
             pltpu.VMEM((VAL_DIM, KEY_DIM), BF16),

time: 93.3 us -> 86.1 us (0.923)
  Pallas kernels: 91.5 us -> 84.3 us
    pallas_call x1, Pallas kernels: 91.5 us -> 84.3 us  [local(): pl.pallas_call(kernel, out_shape=jax.ShapeDtypeStruct((ROWS, WIDTH), BF16...]
where the time goes in v4:
time: 86.1 us; the launch traced here: 85.9 us
  Pallas kernels  84.3 us (98%)
  local copies, waits for them, and re-layouts  1.62 us (2%)
    pallas_call x1, Pallas kernels, local(): pl.pallas_call(kernel, out_shape=jax.ShapeDtypeStruct((ROWS, WIDTH), BF16...  84.3 us

profile of v4, /device:TPU:1, one launch (start us, length us, event | category | flops | bytes accessed | tf_op | source)
XLA Modules:
  0.0 85.9 jit_solution(12914512624517259292)
XLA Ops:
  0.0 84.3 %shard_map.145 = bf16[48,2048]{1,0:T(8,128)(2,1)} custom-call(bf16[48,2048]{1,0:T(8,128)(2,1)} %tok_h.1, f32[1,2048]{1,0:T(1,128)} %bitcast.9, bf16[32,256]{1,0:T(8,128)(2,1)} %ci_h.1, bf16[32,256]{1,0:T(8,128)(2,1)} %cg_h.1, f32[3,2048]{1,0:T(4,128)} %taps_h.1, bf16[32,128]{1,0:T(8,128)(2,1)} %q_h.1, bf16[32,128]{1,0:T(8,128)(2,1)} %k_h.1, ...), custom_call_target="tpu_custom_call" | custom-call | flops 3000000000 | bytes 1000000 | tf_op jit(solution)/shard_map/pallas_call | solution.py:541
  84.3 1.6 %copy.17 = bf16[48,2048]{1,0:T(8,128)(2,1)} copy(bf16[48,2048]{1,0:T(8,128)(2,1)} %shard_map.145) | data formatting | bytes 393216

commit v5 on v4

--- a/solution.py
+++ b/solution.py
@@ -67,7 +67,7 @@
     tok_h, gain_h, ci_h, cg_h, taps_h, q_h, k_h, v_h, dd_h, du_h, db_h, de_h, hg_h, co_h, vo_h,
     out,
     tok, norm_gain, taps, ddown, dup, dbias, dextra, hgain,
-    WA, WB, WC, T, SS, R1, M2, NEAR, M4, R2, M3, IF, IB, CI, CP, HP, HN, XC, PO, PS, PR, XS, XR,
+    WA, WB, WC, T, SS, R1, M2, NEAR, M4, R2, M3, IF, IB, CI, CP, HP, HN, XC, PO, PS, PR, XS, XQ, XP, XR,
     ssem, rsem, lsem,
 ):
     z, y, x, c = (lax.axis_index(a) for a in SP_TP)
@@ -284,7 +284,7 @@
         return array[n * BLOCK : (n + 1) * BLOCK]
 
     def decay():
-        low = mm_nt(T[...], ddown[...]).astype(BF16)
+        low = mm_nt(T[0:LEN, :], ddown[...]).astype(BF16)
         pre = mm(low, dup[:, key_cols]) + dbias[:, key_cols]
         log_sig = jnp.minimum(pre, 0.0) - jnp.log1p(jnp.exp(-jnp.abs(pre)))
         extra = jnp.transpose(jnp.broadcast_to(dextra[...], (KEY_DIM, LEN)))
@@ -313,6 +313,15 @@
     ring_a.stage(4)
     ring_a.column(5, 13)
     token_step(2)
+    for name, device, edge, at_row in (("hp", next_dev, LEN - 16, 15), ("hn", prev_dev, 0, 0)):
+        rows = T[edge : edge + 16, :].astype(F32)[at_row : at_row + 1]
+        arow = lax.broadcasted_iota(jnp.int32, (16, 256), 0)
+        spread = jnp.zeros((16, 256), F32)
+        for i in range(8):
+            spread = jnp.where(arow == i, rows[:, i * 256 : (i + 1) * 256], spread)
+        to = pl.ds(16 if at_row == 0 else 0, 16)
+        CI[to, :] = spread.astype(BF16)
+        send(CI.at[to], HN if at_row == 0 else HP, name, device)
     cumul, before = decay()
     totals = [cumul[(n + 1) * BLOCK - 1 : (n + 1) * BLOCK] for n in range(blocks)]
     offsets = [jnp.zeros((1, KEY_DIM), F32)]
@@ -333,7 +342,7 @@
     weights_step(5, fan=False)
     ring_a.last_column()
 
-    normed = T[...]
+    normed = T[0:LEN, :]
     kv = mm(normed, WA[...])
     key_f = kv[:, :KEY_DIM].astype(BF16).astype(F32)
     value = kv[:, KEY_DIM:].astype(BF16)
@@ -407,15 +416,6 @@
     late_fan(4, 12)
     weights_step(9)
     late_fan(5, 13)
-    ring_b.finish()
-    qcg = mm(normed, WB[...])
-    query_f = (qcg[:, :KEY_DIM] * (1.0 / math.sqrt(KEY_DIM))).astype(BF16).astype(F32)
-    conv_in = qcg[:, KEY_DIM : KEY_DIM + 256].astype(BF16)
-    gate = qcg[:, KEY_DIM + 256 :].astype(BF16).astype(F32)
-    CI[...] = conv_in
-    CP[8 : 8 + LEN, :] = conv_in.astype(F32)
-    send(CI.at[pl.ds(LEN - 16, 16)], HP, "hp", next_dev)
-    send(CI.at[pl.ds(0, 16)], HN, "hn", prev_dev)
     for d in range(2, NZ, 2):
         arrived(R2.at[depth(-d)], ("s2", d))
     sum_f = jnp.zeros((64, KEY_DIM), F32)
@@ -444,6 +444,21 @@
         send(M3.at[answer(d, 1)], IB.at[quarter()], ("s3b", d), at(dy=d))
     IF[quarter(), :] = M3[answer(0, 0), :]
     IB[quarter(), :] = M3[answer(0, 1), :]
+    ring_b.finish()
+    arrived(HP, "hp")
+    arrived(HN, "hn")
+    for i in range(8):
+        seg = pl.ds(i * 256, 256)
+        arow = lax.broadcasted_iota(jnp.int32, (16, 256), 0)
+        row_p = jnp.where(s > 0, HP[i : i + 1, :].astype(F32), 0.0)
+        row_n = jnp.where(s < NZ * NY - 1, HN[i : i + 1, :].astype(F32), 0.0)
+        T[pl.ds(LEN, 16), seg] = jnp.where(arow == 0, row_p, jnp.where(arow == 1, row_n, 0.0)).astype(BF16)
+    conv_in = mm(T[...], WB[:, 128:384]).astype(BF16).astype(F32)
+    CP[8 : 8 + LEN, :] = conv_in[:LEN]
+    CP[7:8, :] = conv_in[LEN : LEN + 1]
+    CP[8 + LEN : 9 + LEN, :] = conv_in[LEN + 1 : LEN + 2]
+    query_f = (mm(normed, WB[:, 0:128]) * (1.0 / math.sqrt(KEY_DIM))).astype(BF16).astype(F32)
+    gate = mm(normed, WB[:, 384:640]).astype(BF16).astype(F32)
     lower = lax.broadcasted_iota(jnp.int32, (BLOCK, BLOCK), 0) >= lax.broadcasted_iota(jnp.int32, (BLOCK, BLOCK), 1)
     upper = lax.broadcasted_iota(jnp.int32, (BLOCK, BLOCK), 0) <= lax.broadcasted_iota(jnp.int32, (BLOCK, BLOCK), 1)
     within = []
@@ -476,12 +491,6 @@
         [part(query_f, n) * jnp.exp(suffix[n] + (totals[n] - part(before, n))) for n in range(blocks)], axis=0
     ).astype(BF16)
 
-    arrived(HP, "hp")
-    arrived(HN, "hn")
-    first = HP[...].astype(F32)[15:16]
-    last = HN[...].astype(F32)[0:1]
-    CP[7:8, :] = jnp.where(s > 0, first, 0.0)
-    CP[8 + LEN : 9 + LEN, :] = jnp.where(s < NZ * NY - 1, last, 0.0)
     tap = taps[:, val_cols]
     mixed = CP[7 : 7 + LEN, :] * tap[0:1] + CP[8 : 8 + LEN, :] * tap[1:2] + CP[9 : 9 + LEN, :] * tap[2:3]
     XC[:, 0:256] = (mixed * (gate * (1.0 / (1.0 + jnp.exp(-gate))))).astype(BF16)
@@ -506,14 +515,31 @@
         PS[rows4(n), :] = mm_nt(there, WC[n * piece : (n + 1) * piece, :]).astype(BF16)
         send(PS.at[rows4(n)], PR.at[rows4(n)], ("pr", n), at(flip=True))
 
+    side = piece // 2
+    near, far_side = pl.ds(0, side), pl.ds(side, side)
+
     def x_send(n):
         mine = mm_nt(here, WC[n * piece : (n + 1) * piece, :])
         arrived(PR.at[rows4(n)], ("pr", n))
         both = mine + PR[rows4(n), :].astype(F32)
         XS[rows4(n), :] = both.astype(BF16)
-        for i in range(3):
-            send(XS.at[rows4(n, i, 1)], XR.at[rows4(n, i, 1)], ("xr", n, i), at(dx=order[i]))
-        PO[pl.ds(n * ROWS, ROWS), :] = both[3 * ROWS :]
+        send(XS.at[rows4(n, 0, 1), near], XQ.at[rows2(n, 0)], ("xq", n, 0), at(dx=1))
+        send(XS.at[rows4(n, 0, 1), far_side], XQ.at[rows2(n, 1)], ("xq", n, 1), at(dx=-1))
+        send(XS.at[rows4(n, 1, 1), far_side], XR.at[rows2(n, 0), far_side], ("xr", n, 0), at(dx=1))
+        send(XS.at[rows4(n, 2, 1), near], XR.at[rows2(n, 1), near], ("xr", n, 1), at(dx=-1))
+        PO[pl.ds(n * ROWS * 3, ROWS * 3), :] = both[ROWS:]
+
+    def rows2(n, i):
+        return pl.ds((n * 2 + i) * ROWS, ROWS)
+
+    def x_pass(n):
+        base = n * ROWS * 3
+        arrived(XQ.at[rows2(n, 0)], ("xq", n, 0))
+        XP[rows2(n, 0), :] = (PO[base : base + ROWS, 0:side] + XQ[rows2(n, 0), :].astype(F32)).astype(BF16)
+        send(XP.at[rows2(n, 0)], XR.at[rows2(n, 0), near], ("xs", n, 0), at(dx=1))
+        arrived(XQ.at[rows2(n, 1)], ("xq", n, 1))
+        XP[rows2(n, 1), :] = (PO[base + ROWS : base + 2 * ROWS, side:] + XQ[rows2(n, 1), :].astype(F32)).astype(BF16)
+        send(XP.at[rows2(n, 1)], XR.at[rows2(n, 1), far_side], ("xs", n, 1), at(dx=-1))
 
     pair_send(0)
     pair_send(1)
@@ -522,10 +548,14 @@
         if n + 2 < pieces:
             pair_send(n + 2)
     for n in range(pieces):
-        total = PO[n * ROWS : (n + 1) * ROWS, :]
-        for i in (1, 2, 0):
-            arrived(XR.at[rows4(n, i, 1)], ("xr", n, i))
-            total = total + XR[rows4(n, i, 1), :].astype(F32)
+        x_pass(n)
+    for n in range(pieces):
+        total = PO[n * ROWS * 3 + 2 * ROWS : (n + 1) * ROWS * 3, :]
+        arrived(XR.at[rows2(n, 0), far_side], ("xr", n, 0))
+        arrived(XR.at[rows2(n, 1), near], ("xr", n, 1))
+        arrived(XR.at[rows2(n, 0), near], ("xs", n, 0))
+        arrived(XR.at[rows2(n, 1), far_side], ("xs", n, 1))
+        total = total + XR[rows2(n, 0), :].astype(F32) + XR[rows2(n, 1), :].astype(F32)
         out[:, n * piece : (n + 1) * piece] = total.astype(BF16)
 
     for copy in sends:
@@ -540,7 +570,7 @@
     hbm = pl.BlockSpec(memory_space=pl.ANY)
     return pl.pallas_call(
         kernel,
-        out_shape=jax.ShapeDtypeStruct((ROWS, WIDTH), BF16),
+        out_shape=pltpu.VMEM((ROWS, WIDTH), BF16),
         in_specs=[hbm] * 15,
         out_specs=pl.BlockSpec(memory_space=pltpu.VMEM),
         scratch_shapes=[
@@ -555,7 +585,7 @@
             pltpu.VMEM((2048, 384), BF16),
             pltpu.VMEM((2048, 640), BF16),
             pltpu.VMEM((2048, 512), BF16),
-            pltpu.VMEM((LEN, WIDTH), BF16),
+            pltpu.VMEM((LEN + 16, WIDTH), BF16),
             pltpu.VMEM((NY * 144, KEY_DIM), BF16),
             pltpu.VMEM((NY * 144, KEY_DIM), BF16),
             pltpu.VMEM((160, KEY_DIM), BF16),
@@ -565,16 +595,18 @@
             pltpu.VMEM((NY * 128, KEY_DIM), BF16),
             pltpu.VMEM((VAL_DIM, KEY_DIM), BF16),
             pltpu.VMEM((VAL_DIM, KEY_DIM), BF16),
-            pltpu.VMEM((LEN, 256), BF16),
+            pltpu.VMEM((32, 256), BF16),
             pltpu.VMEM((LEN + 16, 256), F32),
             pltpu.VMEM((16, 256), BF16),
             pltpu.VMEM((16, 256), BF16),
             pltpu.VMEM((LEN, 512), BF16),
-            pltpu.VMEM((4 * ROWS, WIDTH // 4), F32),
+            pltpu.VMEM((12 * ROWS, WIDTH // 4), F32),
             pltpu.VMEM((16 * ROWS, WIDTH // 4), BF16),
             pltpu.VMEM((16 * ROWS, WIDTH // 4), BF16),
             pltpu.VMEM((16 * ROWS, WIDTH // 4), BF16),
-            pltpu.VMEM((16 * ROWS, WIDTH // 4), BF16),
+            pltpu.VMEM((8 * ROWS, WIDTH // 8), BF16),
+            pltpu.VMEM((8 * ROWS, WIDTH // 8), BF16),
+            pltpu.VMEM((8 * ROWS, WIDTH // 4), BF16),
             pltpu.SemaphoreType.DMA((N_SEND,)),
             pltpu.SemaphoreType.DMA((N_RECV,)),
             pltpu.SemaphoreType.DMA((15,)),

time: 86.1 us -> 80.2 us (0.931)
  Pallas kernels: 84.3 us -> 79.4 us
  local copies, waits for them, and re-layouts: 1.62 us -> 0.68 us
    pallas_call x1, Pallas kernels: 84.3 us -> 79.4 us  [local(): pl.pallas_call(kernel, out_shape=pltpu.VMEM((ROWS, WIDTH), BF16), in_spec...]
    unnamed x1, local copies, waits for them, and re-layouts: 1.62 us -> 0.68 us
where the time goes in v5:
time: 80.2 us; the launch traced here: 80.1 us
  Pallas kernels  79.4 us (99%)
    pallas_call x1, Pallas kernels, local(): pl.pallas_call(kernel, out_shape=pltpu.VMEM((ROWS, WIDTH), BF16), in_spec...  79.4 us

profile of v5, /device:TPU:1, one launch (start us, length us, event | category | flops | bytes accessed | tf_op | source)
XLA Modules:
  0.0 80.1 jit_solution(1358199090054070059)
XLA Ops:
  0.0 79.4 %shard_map.145 = bf16[48,2048]{1,0:T(8,128)(2,1)S(1)} custom-call(bf16[48,2048]{1,0:T(8,128)(2,1)} %tok_h.1, f32[1,2048]{1,0:T(1,128)} %bitcast.9, bf16[32,256]{1,0:T(8,128)(2,1)} %ci_h.1, bf16[32,256]{1,0:T(8,128)(2,1)} %cg_h.1, f32[3,2048]{1,0:T(4,128)} %taps_h.1, bf16[32,128]{1,0:T(8,128)(2,1)} %q_h.1, bf16[32,128]{1,0:T(8,128)(2,1)} %k_h.1, ...), custom_call_target="tpu_custom_call" | custom-call | flops 3000000000 | bytes 1000000 | tf_op jit(solution)/shard_map/pallas_call | solution.py:571
  79.4 0.7 copy.17

commit v6 on v5

--- a/solution.py
+++ b/solution.py
@@ -105,10 +105,6 @@
     peers += [at(dy=d) for d in range(1, NY)]
     peers += [at(dx=d) for d in range(1, NX)]
     peers += [at(flip=True), next_dev, prev_dev]
-    barrier = pltpu.get_barrier_semaphore()
-    for peer in peers:
-        pl.semaphore_signal(barrier, inc=1, device_id=peer, device_id_type=MESH)
-
     def slot(dz=0, dy=0):
         index = wrap(z + dz, NZ) * NY + wrap(y + dy, NY)
         return pl.ds(pl.multiple_of(index * 32, 32), 32)
@@ -131,6 +127,9 @@
     load(v_h, WA.at[slot(), pl.ds(128, 256)])
     load(tok_h, tok)
     load(gain_h, norm_gain)
+    barrier = pltpu.get_barrier_semaphore()
+    for peer in peers:
+        pl.semaphore_signal(barrier, inc=1, device_id=peer, device_id_type=MESH)
     load(q_h, WB.at[slot(), pl.ds(0, 128)])
     load(ci_h, WB.at[slot(), pl.ds(128, 256)])
     load(cg_h, WB.at[slot(), pl.ds(384, 256)])
@@ -142,14 +141,8 @@
     load(de_h, dextra)
     load(taps_h, taps)
     load(hg_h, hgain)
-    for copy in loads[:4]:
+    for copy in loads[:2]:
         copy.wait()
-    raw_rows = tok[...].astype(F32)
-    scale = lax.rsqrt(jnp.mean(raw_rows * raw_rows, axis=-1, keepdims=True) + EPSILON)
-    T[token_rows(), :] = (raw_rows * scale * norm_gain[...]).astype(BF16)
-    for copy in loads[4:]:
-        copy.wait()
-
     pl.semaphore_wait(barrier, len(peers))
 
     def place(j):
@@ -181,17 +174,18 @@
         def step(self, k, chains=(0, 1), fan=True):
             for chain in chains:
                 for sign in (1, -1):
-                    if sign == -1 and k == 8:
+                    most = 8 if (sign == 1) == (chain == 0) else 7
+                    if k > most:
                         continue
                     arrived(self.W.at[slot(-sign * k, 2 * chain)], (self.tag, chain, sign, k))
-                    if k < (8 if sign == 1 else 7):
+                    if k < most:
                         self.hop(chain, sign, k + 1)
                     if chain == 0 and fan:
                         self.fan_out(k if sign == 1 else 8 + k)
 
         def column(self, *js):
             for j in js:
-                plus = (j % 2 == 0) if j <= 8 else ((j - 8) % 2 == 1)
+                plus = (j % 2 == 0 and j < 8) if j <= 8 else ((j - 8) % 2 == 1)
                 for dy, name in ((-1, "ym"), (1, "yp")):
                     ref = self.W.at[slot(place(j), dy)]
                     arrived(ref, (self.tag, name, j))
@@ -229,6 +223,11 @@
     ring_a.leap(1, 0)
     ring_a.leap(-1, 0)
     ring_a.fan_out(0)
+    for copy in loads[2:]:
+        copy.wait()
+    raw_rows = tok[...].astype(F32)
+    scale = lax.rsqrt(jnp.mean(raw_rows * raw_rows, axis=-1, keepdims=True) + EPSILON)
+    T[token_rows(), :] = (raw_rows * scale * norm_gain[...]).astype(BF16)
     own_rows = T.at[token_rows()]
     send(own_rows, own_rows, "tm", at(dx=1))
     send(own_rows, own_rows, "tp", at(dx=-1))
@@ -495,6 +494,9 @@
     mixed = CP[7 : 7 + LEN, :] * tap[0:1] + CP[8 : 8 + LEN, :] * tap[1:2] + CP[9 : 9 + LEN, :] * tap[2:3]
     XC[:, 0:256] = (mixed * (gate * (1.0 / (1.0 + jnp.exp(-gate))))).astype(BF16)
 
+    early = len(sends) - 6
+    for copy in sends[:early]:
+        copy.wait_send()
     for d in range(1, NY):
         arrived(IF.at[quarter(-d)], ("s3f", d))
         arrived(IB.at[quarter(-d)], ("s3b", d))
@@ -518,22 +520,26 @@
     side = piece // 2
     near, far_side = pl.ds(0, side), pl.ds(side, side)
 
+    def keep(n):
+        PO[rows4(n), :] = mm_nt(here, WC[n * piece : (n + 1) * piece, :])
+
     def x_send(n):
-        mine = mm_nt(here, WC[n * piece : (n + 1) * piece, :])
         arrived(PR.at[rows4(n)], ("pr", n))
-        both = mine + PR[rows4(n), :].astype(F32)
+        both = PO[rows4(n), :] + PR[rows4(n), :].astype(F32)
         XS[rows4(n), :] = both.astype(BF16)
         send(XS.at[rows4(n, 0, 1), near], XQ.at[rows2(n, 0)], ("xq", n, 0), at(dx=1))
         send(XS.at[rows4(n, 0, 1), far_side], XQ.at[rows2(n, 1)], ("xq", n, 1), at(dx=-1))
+        PO[rows4(n, 1, 3), :] = both[ROWS:]
+
+    def x_direct(n):
         send(XS.at[rows4(n, 1, 1), far_side], XR.at[rows2(n, 0), far_side], ("xr", n, 0), at(dx=1))
         send(XS.at[rows4(n, 2, 1), near], XR.at[rows2(n, 1), near], ("xr", n, 1), at(dx=-1))
-        PO[pl.ds(n * ROWS * 3, ROWS * 3), :] = both[ROWS:]
 
     def rows2(n, i):
         return pl.ds((n * 2 + i) * ROWS, ROWS)
 
     def x_pass(n):
-        base = n * ROWS * 3
+        base = (n * 4 + 1) * ROWS
         arrived(XQ.at[rows2(n, 0)], ("xq", n, 0))
         XP[rows2(n, 0), :] = (PO[base : base + ROWS, 0:side] + XQ[rows2(n, 0), :].astype(F32)).astype(BF16)
         send(XP.at[rows2(n, 0)], XR.at[rows2(n, 0), near], ("xs", n, 0), at(dx=1))
@@ -541,16 +547,18 @@
         XP[rows2(n, 1), :] = (PO[base + ROWS : base + 2 * ROWS, side:] + XQ[rows2(n, 1), :].astype(F32)).astype(BF16)
         send(XP.at[rows2(n, 1)], XR.at[rows2(n, 1), far_side], ("xs", n, 1), at(dx=-1))
 
-    pair_send(0)
-    pair_send(1)
+    for n in range(pieces):
+        pair_send(n)
+    for n in range(pieces):
+        keep(n)
     for n in range(pieces):
         x_send(n)
-        if n + 2 < pieces:
-            pair_send(n + 2)
+    for n in range(pieces):
+        x_direct(n)
     for n in range(pieces):
         x_pass(n)
     for n in range(pieces):
-        total = PO[n * ROWS * 3 + 2 * ROWS : (n + 1) * ROWS * 3, :]
+        total = PO[rows4(n, 3, 1), :]
         arrived(XR.at[rows2(n, 0), far_side], ("xr", n, 0))
         arrived(XR.at[rows2(n, 1), near], ("xr", n, 1))
         arrived(XR.at[rows2(n, 0), near], ("xs", n, 0))
@@ -558,7 +566,7 @@
         total = total + XR[rows2(n, 0), :].astype(F32) + XR[rows2(n, 1), :].astype(F32)
         out[:, n * piece : (n + 1) * piece] = total.astype(BF16)
 
-    for copy in sends:
+    for copy in sends[early:]:
         copy.wait_send()
     assert len(sends) <= N_SEND and len(names) <= N_RECV, (len(sends), len(names))
 
@@ -600,7 +608,7 @@
             pltpu.VMEM((16, 256), BF16),
             pltpu.VMEM((16, 256), BF16),
             pltpu.VMEM((LEN, 512), BF16),
-            pltpu.VMEM((12 * ROWS, WIDTH // 4), F32),
+            pltpu.VMEM((16 * ROWS, WIDTH // 4), F32),
             pltpu.VMEM((16 * ROWS, WIDTH // 4), BF16),
             pltpu.VMEM((16 * ROWS, WIDTH // 4), BF16),
             pltpu.VMEM((16 * ROWS, WIDTH // 4), BF16),

time: 80.2 us -> 79.7 us (level)
  no operation moved by 1% of the time
where the time goes in v6:
time: 79.7 us; the launch traced here: 79.6 us
  Pallas kernels  78.9 us (99%)
    pallas_call x1, Pallas kernels, local(): pl.pallas_call(kernel, out_shape=pltpu.VMEM((ROWS, WIDTH), BF16), in_spec...  78.9 us

profile of v6, /device:TPU:1, one launch (start us, length us, event | category | flops | bytes accessed | tf_op | source)
XLA Modules:
  0.0 79.6 jit_solution(4992306021993433625)
XLA Ops:
  0.0 78.9 %shard_map.145 = bf16[48,2048]{1,0:T(8,128)(2,1)S(1)} custom-call(bf16[48,2048]{1,0:T(8,128)(2,1)} %tok_h.1, f32[1,2048]{1,0:T(1,128)} %bitcast.9, bf16[32,256]{1,0:T(8,128)(2,1)} %ci_h.1, bf16[32,256]{1,0:T(8,128)(2,1)} %cg_h.1, f32[3,2048]{1,0:T(4,128)} %taps_h.1, bf16[32,128]{1,0:T(8,128)(2,1)} %q_h.1, bf16[32,128]{1,0:T(8,128)(2,1)} %k_h.1, ...), custom_call_target="tpu_custom_call" | custom-call | flops 3000000000 | bytes 1000000 | tf_op jit(solution)/shard_map/pallas_call | solution.py:579
  78.9 0.7 copy.17

commit v7 on v6

--- a/solution.py
+++ b/solution.py
@@ -149,8 +149,8 @@
         return 0 if j == 0 else (-j if j <= 8 else j - 8)
 
     class Ring:
-        def __init__(self, W, tag):
-            self.W, self.tag = W, tag
+        def __init__(self, W, tag, reach=8):
+            self.W, self.tag, self.reach, self.passed = W, tag, reach, []
 
         def hop(self, chain, sign, k):
             ref = self.W.at[slot(-sign * (k - 1), 2 * chain)]
@@ -174,7 +174,7 @@
         def step(self, k, chains=(0, 1), fan=True):
             for chain in chains:
                 for sign in (1, -1):
-                    most = 8 if (sign == 1) == (chain == 0) else 7
+                    most = min(8 if (sign == 1) == (chain == 0) else 7, self.reach if chain else 8)
                     if k > most:
                         continue
                     arrived(self.W.at[slot(-sign * k, 2 * chain)], (self.tag, chain, sign, k))
@@ -185,6 +185,7 @@
 
         def column(self, *js):
             for j in js:
+                self.passed.append(j)
                 plus = (j % 2 == 0 and j < 8) if j <= 8 else ((j - 8) % 2 == 1)
                 for dy, name in ((-1, "ym"), (1, "yp")):
                     ref = self.W.at[slot(place(j), dy)]
@@ -198,8 +199,11 @@
 
         def finish(self):
             for j in range(16):
-                arrived(self.W.at[slot(place(j), -1)], (self.tag, "ym", j))
-                arrived(self.W.at[slot(place(j), 1)], (self.tag, "yp", j))
+                if j in self.passed:
+                    arrived(self.W.at[slot(place(j), 2)], (self.tag, "y2", j))
+                else:
+                    arrived(self.W.at[slot(place(j), -1)], (self.tag, "ym", j))
+                    arrived(self.W.at[slot(place(j), 1)], (self.tag, "yp", j))
 
     class Jumps(Ring):
         def leap(self, sign, base):
@@ -219,7 +223,7 @@
                         self.leap(sign, k)
                     self.fan_out(k if sign == 1 else 8 + k)
 
-    ring_a, ring_b, ring_c = Jumps(WA, "a"), Ring(WB, "b"), Ring(WC, "c")
+    ring_a, ring_b, ring_c = Jumps(WA, "a"), Ring(WB, "b"), Ring(WC, "c", reach=4)
     ring_a.leap(1, 0)
     ring_a.leap(-1, 0)
     ring_a.fan_out(0)
@@ -360,7 +364,7 @@
     for d in range(1, NY):
         send(SS.at[message(d)], R1.at[message()], ("s1", d), at(dy=d))
 
-    late_fan(0, 1, 9)
+    late_fan(5, 13, 0)
     weights_step(6)
     for d in range(1, NY):
         arrived(R1.at[message(-d)], ("s1", d))
@@ -394,7 +398,7 @@
     R2[depth(), :] = M2[0:80, :]
     send(M2.at[pl.ds(0, 80)], NEAR.at[pl.ds(0, 80)], "s2f", at(dz=1))
     send(M2.at[pl.ds(80, 80)], NEAR.at[pl.ds(80, 80)], "s2b", at(dz=-1))
-    late_fan(2, 10)
+    late_fan(1, 9)
     weights_step(7)
     arrived(NEAR.at[pl.ds(0, 80)], "s2f")
     arrived(NEAR.at[pl.ds(80, 80)], "s2b")
@@ -410,11 +414,13 @@
         start = pl.multiple_of(((z + d) // NZ) * 80, 16)
         send(M4.at[pl.ds(start, 80)], R2.at[depth()], ("s2", d), at(dz=d))
 
+    late_fan(2, 10)
+    weights_step(8)
+    ring_c.column(5, 13)
     late_fan(3, 11)
-    weights_step(8)
+    weights_step(9)
+    ring_c.column(6, 14, 7, 15)
     late_fan(4, 12)
-    weights_step(9)
-    late_fan(5, 13)
     for d in range(2, NZ, 2):
         arrived(R2.at[depth(-d)], ("s2", d))
     sum_f = jnp.zeros((64, KEY_DIM), F32)
@@ -443,6 +449,7 @@
         send(M3.at[answer(d, 1)], IB.at[quarter()], ("s3b", d), at(dy=d))
     IF[quarter(), :] = M3[answer(0, 0), :]
     IB[quarter(), :] = M3[answer(0, 1), :]
+    ring_c.column(8)
     ring_b.finish()
     arrived(HP, "hp")
     arrived(HN, "hn")

time: 79.7 us -> 79.3 us (level)
  no operation moved by 1% of the time
where the time goes in v7:
time: 79.3 us; the launch traced here: 79.2 us
  Pallas kernels  78.5 us (99%)
    pallas_call x1, Pallas kernels, local(): pl.pallas_call(kernel, out_shape=pltpu.VMEM((ROWS, WIDTH), BF16), in_spec...  78.5 us

profile of v7, /device:TPU:1, one launch (start us, length us, event | category | flops | bytes accessed | tf_op | source)
XLA Modules:
  0.0 79.2 jit_solution(6226083667645884288)
XLA Ops:
  0.0 78.5 %shard_map.145 = bf16[48,2048]{1,0:T(8,128)(2,1)S(1)} custom-call(bf16[48,2048]{1,0:T(8,128)(2,1)} %tok_h.1, f32[1,2048]{1,0:T(1,128)} %bitcast.9, bf16[32,256]{1,0:T(8,128)(2,1)} %ci_h.1, bf16[32,256]{1,0:T(8,128)(2,1)} %cg_h.1, f32[3,2048]{1,0:T(4,128)} %taps_h.1, bf16[32,128]{1,0:T(8,128)(2,1)} %q_h.1, bf16[32,128]{1,0:T(8,128)(2,1)} %k_h.1, ...), custom_call_target="tpu_custom_call" | custom-call | flops 3000000000 | bytes 1000000 | tf_op jit(solution)/shard_map/pallas_call | solution.py:586
  78.5 0.7 copy.17

commit v8 on v7

--- a/solution.py
+++ b/solution.py
@@ -223,7 +223,7 @@
                         self.leap(sign, k)
                     self.fan_out(k if sign == 1 else 8 + k)
 
-    ring_a, ring_b, ring_c = Jumps(WA, "a"), Ring(WB, "b"), Ring(WC, "c", reach=4)
+    ring_a, ring_b, ring_c = Jumps(WA, "a"), Ring(WB, "b"), Ring(WC, "c", reach=3)
     ring_a.leap(1, 0)
     ring_a.leap(-1, 0)
     ring_a.fan_out(0)
@@ -364,7 +364,7 @@
     for d in range(1, NY):
         send(SS.at[message(d)], R1.at[message()], ("s1", d), at(dy=d))
 
-    late_fan(5, 13, 0)
+    late_fan(4, 12, 5, 13)
     weights_step(6)
     for d in range(1, NY):
         arrived(R1.at[message(-d)], ("s1", d))
@@ -398,7 +398,7 @@
     R2[depth(), :] = M2[0:80, :]
     send(M2.at[pl.ds(0, 80)], NEAR.at[pl.ds(0, 80)], "s2f", at(dz=1))
     send(M2.at[pl.ds(80, 80)], NEAR.at[pl.ds(80, 80)], "s2b", at(dz=-1))
-    late_fan(1, 9)
+    late_fan(0, 1, 9)
     weights_step(7)
     arrived(NEAR.at[pl.ds(0, 80)], "s2f")
     arrived(NEAR.at[pl.ds(80, 80)], "s2b")
@@ -416,11 +416,10 @@
 
     late_fan(2, 10)
     weights_step(8)
-    ring_c.column(5, 13)
+    ring_c.column(4, 12, 5, 13)
     late_fan(3, 11)
     weights_step(9)
     ring_c.column(6, 14, 7, 15)
-    late_fan(4, 12)
     for d in range(2, NZ, 2):
         arrived(R2.at[depth(-d)], ("s2", d))
     sum_f = jnp.zeros((64, KEY_DIM), F32)

time: 79.3 us -> 79.7 us (level)
  no operation moved by 1% of the time
where the time goes in v8:
time: 79.7 us; the launch traced here: 79.6 us
  Pallas kernels  78.9 us (99%)
    pallas_call x1, Pallas kernels, local(): pl.pallas_call(kernel, out_shape=pltpu.VMEM((ROWS, WIDTH), BF16), in_spec...  78.9 us

profile of v8, /device:TPU:1, one launch (start us, length us, event | category | flops | bytes accessed | tf_op | source)
XLA Modules:
  0.0 79.6 jit_solution(13162605543088616064)
XLA Ops:
  0.0 78.9 %shard_map.145 = bf16[48,2048]{1,0:T(8,128)(2,1)S(1)} custom-call(bf16[48,2048]{1,0:T(8,128)(2,1)} %tok_h.1, f32[1,2048]{1,0:T(1,128)} %bitcast.9, bf16[32,256]{1,0:T(8,128)(2,1)} %ci_h.1, bf16[32,256]{1,0:T(8,128)(2,1)} %cg_h.1, f32[3,2048]{1,0:T(4,128)} %taps_h.1, bf16[32,128]{1,0:T(8,128)(2,1)} %q_h.1, bf16[32,128]{1,0:T(8,128)(2,1)} %k_h.1, ...), custom_call_target="tpu_custom_call" | custom-call | flops 3000000000 | bytes 1000000 | tf_op jit(solution)/shard_map/pallas_call | solution.py:585
  78.9 0.7 copy.17
